TPU v7x, 32 devices: a whole 2x2x4 slice. The times are simulated.
32 devices in a mesh: ep: 16 (over z, y, x), tp: 2 (over core).
Axes of the slice: x: 2, y: 2, z: 4, core: 2. Of those that a mesh axis runs over, the one named last changes fastest.
Arguments:
- tokens: bfloat16 [1024, 2048], P('ep', 'tp'), may hold values from -6 to 6
- sequence_state_real: float32 [1024, 128, 64], P('ep', 'tp'), may hold values from -4 to 4
- sequence_state_imaginary: float32 [1024, 128, 64], P('ep', 'tp'), may hold values from -4 to 4
- mixer_norm_gain: float32 [2048], replicated, may hold values from 0.1 to 1.9
- expert_norm_gain: float32 [2048], replicated, may hold values from 0.1 to 1.9
- rate: float32 [128, 64], P('tp'), may hold values from 0.1 to 4
- freq: float32 [128, 64], P('tp'), may hold values from -3 to 3
- log_group_step: float32 [128], P('tp'), may hold values from -3 to 0
- input_map_real: float32 [128, 64, 16], P('tp'), may hold values from -1 to 1
- input_map_imaginary: float32 [128, 64, 16], P('tp'), may hold values from -1 to 1
- output_map_real: float32 [128, 16, 64], P('tp'), may hold values from -0.75 to 0.75
- output_map_imaginary: float32 [128, 16, 64], P('tp'), may hold values from -0.75 to 0.75
- skip: float32 [2048], P('tp'), may hold values from -4 to 4
- mixer_value_weight: bfloat16 [2048, 2048], P('tp'), may hold values from -0.125 to 0.125
- mixer_gate_weight: bfloat16 [2048, 2048], P('tp'), may hold values from -0.125 to 0.125
- group_router_weight: bfloat16 [2048, 4], replicated, may hold values from -0.125 to 0.125
- expert_router_weight: bfloat16 [2048, 16], replicated, may hold values from -0.125 to 0.125
- dense_blend_weight: float32 [2048], replicated, may hold values from -0.125 to 0.125
- routes: int32 [1024, 2], P('ep'), may hold values from 0 to 15, all different within a row; in each aligned block of 64 rows (0 to 63, 64 to 127, ...) at most 16 rows name the same one
- expert_gate_weight: bfloat16 [16, 2048, 1024], P('ep', None, 'tp'), may hold values from -0.125 to 0.125
- expert_up_weight: bfloat16 [16, 2048, 1024], P('ep', None, 'tp'), may hold values from -0.125 to 0.125
- expert_down_weight: bfloat16 [16, 1024, 2048], P('ep', 'tp'), may hold values from -0.1875 to 0.1875
- shared_gate_weight: bfloat16 [2048, 2048], P('tp', 'ep'), may hold values from -0.125 to 0.125
- shared_up_weight: bfloat16 [2048, 2048], P('tp', 'ep'), may hold values from -0.125 to 0.125
- shared_down_weight: bfloat16 [2048, 2048], P(None, 'tp'), may hold values from -0.125 to 0.125
Outputs:
- result: bfloat16 [1024, 2048], P('ep', 'tp')
- next_re: float32 [1024, 128, 64], P('ep', 'tp')
- next_im: float32 [1024, 128, 64], P('ep', 'tp')
Inputs may be any that keep to these rules, and one draw needn't show every extreme that they name: `routes`: each row names 2 different experts. Among the rows of one device no expert is named more than 16 times, and in every draw some expert is named exactly 16 times by some device's rows.
All inputs are finite; a program needn't handle non-finite values.
Results may differ from a plain program's by a relative error of at most 0.017.
Values may be sent and summed in bfloat16 or wider, within the bound.
A program may use at most 128 MiB of HBM per device.

v0:
```python
import jax
import jax.numpy as jnp
from jax import lax
from jax.sharding import PartitionSpec as P

NG = 4


EPS = 1e-06
PRECISION_MAX = lax.Precision.HIGHEST


def state_factors(rate, freq, log_group_step, input_map_real, input_map_imaginary):
    step_size = jnp.exp(log_group_step)[:, None]
    magnitude = jnp.exp(-rate * step_size)
    abar_re = magnitude * jnp.cos(freq * step_size)
    abar_im = magnitude * jnp.sin(freq * step_size)
    denom = rate * rate + freq * freq
    shift_re = abar_re - 1.0
    fac_re = (abar_im * freq - shift_re * rate) / denom
    fac_im = -(abar_im * rate + shift_re * freq) / denom
    bbar_re = fac_re[:, :, None] * input_map_real - fac_im[:, :, None] * input_map_imaginary
    bbar_im = fac_re[:, :, None] * input_map_imaginary + fac_im[:, :, None] * input_map_real
    return (abar_re, abar_im, bbar_re, bbar_im)


def state_step(
    normed,
    sequence_state_real,
    sequence_state_imaginary,
    factors,
    output_map_real,
    output_map_imaginary,
    skip,
):
    abar_re, abar_im, bbar_re, bbar_im = factors
    groups = abar_re.shape[0]
    inputs = normed.astype(jnp.float32)
    grouped = inputs.reshape(inputs.shape[0], groups, -1)
    drive_re = jnp.einsum("tgc,gpc->tgp", grouped, bbar_re, precision=PRECISION_MAX)
    drive_im = jnp.einsum("tgc,gpc->tgp", grouped, bbar_im, precision=PRECISION_MAX)
    fresh_real = abar_re * sequence_state_real - abar_im * sequence_state_imaginary + drive_re
    fresh_imaginary = abar_re * sequence_state_imaginary + abar_im * sequence_state_real + drive_im
    state_readout = jnp.einsum("dor,zdr->zdo", output_map_real, fresh_real, precision=PRECISION_MAX)
    state_readout = state_readout - jnp.einsum(
        "dor,zdr->zdo", output_map_imaginary, fresh_imaginary, precision=PRECISION_MAX
    )
    mixed = state_readout.reshape(inputs.shape) + skip * inputs
    return (mixed, fresh_real, fresh_imaginary)


def pair_product(left, first_map, second_map):
    first = jnp.dot(left, first_map, preferred_element_type=jnp.float32)
    second = jnp.dot(left, second_map, preferred_element_type=jnp.float32)
    return jnp.concatenate([first, second], axis=1)


def shards(
    tokens,
    sequence_state_real,
    sequence_state_imaginary,
    mixer_norm_gain,
    expert_norm_gain,
    rate,
    freq,
    log_group_step,
    input_map_real,
    input_map_imaginary,
    output_map_real,
    output_map_imaginary,
    skip,
    mixer_value_weight,
    mixer_gate_weight,
    group_router_weight,
    expert_router_weight,
    dense_blend_weight,
    routes,
    expert_gate_weight,
    expert_up_weight,
    expert_down_weight,
    shared_gate_weight,
    shared_up_weight,
    shared_down_weight,
):
    seq_rows, half_width = tokens.shape
    width = 2 * half_width
    column_start = lax.axis_index("tp") * half_width

    def own_rows(values):
        return lax.dynamic_slice_in_dim(values, column_start, half_width, 0)

    float_tokens = tokens.astype(jnp.float32)
    square_sum = lax.psum(jnp.sum(float_tokens * float_tokens, axis=1), "tp")
    first_scale = lax.rsqrt(square_sum / width + EPS)[:, None]
    normed = (float_tokens * first_scale * own_rows(mixer_norm_gain)).astype(jnp.bfloat16)
    factors = state_factors(rate, freq, log_group_step, input_map_real, input_map_imaginary)
    mixed, next_re, next_im = state_step(
        normed,
        sequence_state_real,
        sequence_state_imaginary,
        factors,
        output_map_real,
        output_map_imaginary,
        skip,
    )
    activated = jax.nn.gelu(mixed).astype(jnp.bfloat16)
    value_part = jnp.dot(activated, mixer_value_weight, preferred_element_type=jnp.float32)
    gate_part = jnp.dot(activated, mixer_gate_weight, preferred_element_type=jnp.float32)
    stacked = jnp.stack([value_part, gate_part], axis=1)
    mix_sum = lax.psum_scatter(
        stacked.astype(jnp.bfloat16), "tp", scatter_dimension=2, tiled=True
    ).astype(jnp.float32)
    mix_half = (mix_sum[:, 0] * jax.nn.sigmoid(mix_sum[:, 1])).astype(jnp.bfloat16)
    hidden = (float_tokens + mix_half.astype(jnp.float32)).astype(jnp.bfloat16)
    hidden_f32 = hidden.astype(jnp.float32)
    scaled = hidden_f32 * own_rows(expert_norm_gain)
    router_map = jnp.concatenate(
        [own_rows(group_router_weight), own_rows(expert_router_weight)], axis=1
    ).astype(jnp.float32)
    blend_map = own_rows(dense_blend_weight)
    hidden_squares = jnp.sum(hidden_f32 * hidden_f32, axis=1)
    total_squares = lax.psum(hidden_squares, "tp")
    inverse = lax.rsqrt(total_squares / width + EPS)[:, None]
    normal_rows = scaled * inverse
    raw_part = jnp.dot(normal_rows, router_map, precision=PRECISION_MAX)
    blend_part = jnp.dot(normal_rows, blend_map, precision=PRECISION_MAX)
    logits, blend_logit = lax.psum((raw_part, blend_part), "tp")
    hnorm = (scaled * inverse).astype(jnp.bfloat16)
    experts = expert_router_weight.shape[1]
    top_count = routes.shape[1]
    per_group = experts // NG
    group_prob = jax.nn.softmax(logits[:, :NG], axis=-1)
    expert_logits = logits[:, NG:]
    expert_hits = routes[:, :, None] == jnp.arange(experts, dtype=jnp.int32)[None, None, :]
    chosen = jnp.sum(jnp.where(expert_hits, expert_logits[:, None, :], 0.0), axis=2)
    group_hits = (routes // per_group)[:, :, None] == jnp.arange(NG, dtype=jnp.int32)[None, None, :]
    group_sel = jnp.sum(jnp.where(group_hits, group_prob[:, None, :], 0.0), axis=2)
    weights = jax.nn.softmax(chosen, axis=1) * group_sel
    full_rows = lax.all_gather(hnorm, "tp", axis=1, tiled=True)
    capacity = max(2, 2 * seq_rows * top_count // experts)
    flat_routes = routes.reshape(-1)
    matches = (flat_routes[:, None] == jnp.arange(experts, dtype=jnp.int32)[None, :]).astype(
        jnp.int32
    )
    slot_rank = jnp.sum(jnp.cumsum(matches, axis=0) * matches, axis=1) - 1
    slot_target = flat_routes * capacity + slot_rank
    dispatch = slot_target[None, :] == jnp.arange(experts * capacity, dtype=jnp.int32)[:, None]
    dispatch_rows = jnp.sum(
        dispatch.reshape(experts * capacity, seq_rows, top_count).astype(jnp.float32), axis=2
    )
    outgoing = jnp.dot(
        dispatch_rows.astype(jnp.bfloat16), full_rows, preferred_element_type=jnp.float32
    )
    outgoing = outgoing.astype(jnp.bfloat16).reshape(experts, capacity, width)
    received = lax.all_to_all(outgoing, "ep", split_axis=0, concat_axis=0, tiled=True)
    sources = received.shape[0]
    items = received.shape[1]
    token_rows = received.reshape(sources * items, width)
    gate_e = jnp.dot(token_rows, expert_gate_weight[0], preferred_element_type=jnp.float32)
    expert_up_rows = jnp.dot(token_rows, expert_up_weight[0], preferred_element_type=jnp.float32)
    inner = (jax.nn.silu(gate_e) * expert_up_rows).astype(jnp.bfloat16)
    part_out = jnp.dot(inner, expert_down_weight[0], preferred_element_type=jnp.float32)
    total = lax.psum_scatter(part_out.astype(jnp.bfloat16), "tp", scatter_dimension=1, tiled=True)
    finished = total.reshape(sources, items, half_width)
    returned = lax.all_to_all(finished, "ep", split_axis=0, concat_axis=0, tiled=True)
    returned_flat = returned.reshape(experts * capacity, half_width)
    picked = returned_flat[slot_target].reshape(seq_rows, top_count, half_width).astype(jnp.float32)
    routed = jnp.sum(weights[:, :, None] * picked, axis=1)
    partial_dense = pair_product(
        lax.all_gather(hnorm, "ep", axis=0, tiled=True), shared_gate_weight, shared_up_weight
    )
    dense_sum = lax.psum(partial_dense.astype(jnp.bfloat16), "tp").astype(jnp.float32)
    dense_cols = shared_gate_weight.shape[1]
    inner_cols = (jax.nn.silu(dense_sum[:, :dense_cols]) * dense_sum[:, dense_cols:]).astype(
        jnp.bfloat16
    )
    dense_inner = lax.all_to_all(inner_cols, "ep", split_axis=0, concat_axis=1, tiled=True)
    dense_out = jnp.dot(dense_inner, shared_down_weight, preferred_element_type=jnp.float32)
    result = hidden_f32 + routed + jax.nn.sigmoid(blend_logit)[:, None] * dense_out
    return (result.astype(jnp.bfloat16), next_re, next_im)


def solution(mesh):
    placed = (
        P("ep", "tp"),
        P("ep", "tp", None),
        P("ep", "tp", None),
        P(),
        P(),
        P("tp", None),
        P("tp", None),
        P("tp"),
        P("tp", None, None),
        P("tp", None, None),
        P("tp", None, None),
        P("tp", None, None),
        P("tp"),
        P("tp", None),
        P("tp", None),
        P(),
        P(),
        P(),
        P("ep", None),
        P("ep", None, "tp"),
        P("ep", None, "tp"),
        P("ep", "tp", None),
        P("tp", "ep"),
        P("tp", "ep"),
        P(None, "tp"),
    )
    return jax.shard_map(
        shards,
        mesh=mesh,
        in_specs=placed,
        out_specs=(P("ep", "tp"), P("ep", "tp", None), P("ep", "tp", None)),
        check_vma=False,
    )
```

profile of v0, /device:TPU:0, one launch (start us, length us, event | category | flops | bytes accessed | tf_op | source)
XLA Modules:
  0.0 187.7 jit_solution(3510667995029894204)
XLA Ops:
  7.2 3.5 %copy.64 = f32[64,64,64]{0,2,1:T(8,128)} copy(f32[64,64,64]{2,1,0:T(8,128)} %param.27) | data formatting | bytes 2097152 | tf_op args[2]
  10.7 3.4 %copy.63 = f32[64,64,64]{0,2,1:T(8,128)} copy(f32[64,64,64]{2,1,0:T(8,128)} %param.26) | data formatting | bytes 2097152 | tf_op args[1]
  14.3 2.6 %psum.35 = f32[64]{0:T(128)S(1)} all-reduce(f32[64]{0:T(128)S(1)} %fusion.29), channel_id=1, replica_groups=mesh['ep'=16,'tp'=2] {'tp'}, use_global_device_ids=true, to_apply=%region_1.0 | all-reduce | flops 64 | bytes 512 | tf_op jit(solution)/shard_map/psum | solution.py:93
  16.9 0.8 fusion.31
  17.7 1.1 copy.65
  18.8 1.0 fusion.68
  19.8 4.9 %bitcast_add_fusion.1 = f32[64,64,64]{0,2,1:T(8,128)S(1)} fusion(f32[64,64,64]{0,2,1:T(8,128)} %copy.64, f32[64,64,64]{0,2,1:T(8,128)} %copy.63, bf16[64,64,16]{0,2,1:T(8,128)(2,1)S(1)} %bitcast.75, f32[64,64]{1,0:T(8,128)S(1)} %get-tuple-element.17, f32[64,64]{1,0:T(8,128)S(1)} %get-tuple-element.18, f32[64,64,16]{1,2,0:T(8,128)S(1)} %copy-done.7, ...), kind=kOutput, calls=%fused_computation.13 | convolution fusion | flops 51576832 | bytes 3866624 | tf_op jit(solution)/shard_map/tgc,gpc->tgp/dot_general | solution.py:40
  24.8 3.2 %bitcast_add_fusion = f32[64,64,64]{0,2,1:T(8,128)S(1)} fusion(f32[64,64,64]{0,2,1:T(8,128)S(1)} %copy-done.4, f32[64,64,64]{0,2,1:T(8,128)S(1)} %copy-done.3, bf16[64,64,16]{0,2,1:T(8,128)(2,1)S(1)} %bitcast.76, f32[64,64]{1,0:T(8,128)S(1)} %get-tuple-element.17, f32[64,64]{1,0:T(8,128)S(1)} %get-tuple-element.18, f32[64,64,16]{1,2,0:T(8,128)S(1)} %copy-done.8, ...), kind=kOutput, calls=%fused_computation.12 | convolution fusion | flops 51576832 | bytes 3866624 | tf_op jit(solution)/shard_map/tgc,gpc->tgp/dot_general | solution.py:41
  28.1 1.9 %fusion.77 = f32[64,64,16]{1,2,0:T(8,128)S(1)} fusion(f32[64,64,64]{0,2,1:T(8,128)S(1)} %bitcast_add_fusion.1, f32[64,16,64]{2,1,0:T(8,128)S(1)} %copy-done.11), kind=kOutput, calls=%fused_computation.123 | convolution fusion | flops 50331648 | bytes 1572864 | tf_op jit(solution)/shard_map/dor,zdr->zdo/dot_general | solution.py:44
  30.0 1.9 %convolution_subtract_fusion = f32[64,64,16]{1,2,0:T(8,128)S(1)} fusion(f32[64,64,16]{1,2,0:T(8,128)S(1)} %fusion.77, f32[64,64,64]{0,2,1:T(8,128)S(1)} %bitcast_add_fusion, f32[64,16,64]{2,1,0:T(8,128)S(1)} %copy-done.10), kind=kOutput, calls=%fused_computation.15 | convolution fusion | flops 50397184 | bytes 1835008 | tf_op jit(solution)/shard_map/dor,zdr->zdo/dot_general | solution.py:45
  31.9 0.2 copy.70
  32.1 3.3 %fusion.1 = bf16[64,1,2048]{2,0,1:T(8,128)(2,1)S(1)} fusion(bf16[1024,2048]{1,0:T(8,128)(2,1)} %param.39, f32[64,1024]{1,0:T(8,128)S(1)} %copy.70, f32[1024]{0:T(1024)S(1)} %copy-done.14, f32[1024]{0:T(1024)S(1)} %dynamic_slice.15, f32[64]{0:T(128)S(1)} %add_rsqrt_fusion.1, bf16[64,1024]{1,0:T(8,128)(2,1)S(1)} %copy-done.6), kind=kOutput, calls=%fused_computation.6 | convolution fusion | flops 269615104 | bytes 4858112 | tf_op jit(solution)/shard_map/dot_general | solution.py:108
  35.6 1.0 fusion
  36.6 0.8 pad_maximum_fusion
  37.8 10.3 %reduce-scatter.3.cloned.1.call-done = bf16[64,2,1024]{2,0,1:T(8,128)(2,1)} async-done(((bf16[64,2,2048]{2,0,1:T(8,128)(2,1)}), bf16[64,2,1024]{2,0,1:T(8,128)(2,1)}) %reduce-scatter.3.cloned.1.call-update) | async-done | bytes 262160 | tf_op jit(solution)/shard_map/reduce_scatter | solution.py:110
  48.1 1.0 convert_element_type.70
  49.1 0.2 fusion.46
  49.3 2.5 %psum.36 = f32[64]{0:T(128)S(1)} all-reduce(f32[64]{0:T(128)S(1)} %get-tuple-element.14), channel_id=1, replica_groups=mesh['ep'=16,'tp'=2] {'tp'}, use_global_device_ids=true, to_apply=%region_4.0 | all-reduce | flops 64 | bytes 512 | tf_op jit(solution)/shard_map/psum | solution.py:122
  51.8 0.7 fusion.43
  52.7 0.2 reduce_window_sum.11
  52.8 0.2 select_reduce_fusion
  53.4 2.3 %all_gather.6 = bf16[64,2048]{1,0:T(8,128)(2,1)S(1)} all-gather(bf16[64,1024]{1,0:T(8,128)(2,1)} %fusion.43), channel_id=1, replica_groups=mesh['ep'=16,'tp'=2] {'tp'}, dimensions={1}, use_global_device_ids=true | all-gather | bytes 393216 | tf_op jit(solution)/shard_map/all_gather | solution.py:139
  55.7 0.4 convolution_convert_fusion.1
  56.2 41.0 %all_to_all.29 = bf16[16,16,2048]{2,1,0:T(8,128)(2,1)S(1)} all-to-all(bf16[16,16,2048]{2,1,0:T(8,128)(2,1)S(1)} %bitcast.74), channel_id=1, replica_groups=mesh['ep'=16,'tp'=2] {'ep'}, dimensions={0} | all-to-all | bytes 2097152 | tf_op jit(solution)/shard_map/all_to_all | solution.py:155
  97.2 1.0 copy-done.9
  98.2 0.7 fusion.5
  98.9 4.2 %convolution_convert_fusion = bf16[256,2048]{1,0:T(8,128)(2,1)} fusion(bf16[1,512,2048]{2,1,0:T(8,128)(2,1)S(1)} %copy-done, bf16[256,2048]{1,0:T(8,128)(2,1)} %bitcast.79, bf16[1,2048,512]{2,1,0:T(8,128)(2,1)} %param.45, f32[256,512]{1,0:T(8,128)S(1)} %fusion.5), kind=kOutput, calls=%fused_computation.1 | convolution fusion | flops 1075052544 | bytes 6815744 | tf_op jit(solution)/shard_map/dot_general | solution.py:162
  103.1 3.8 %copy.77 = f32[64,64,64]{2,1,0:T(8,128)} copy(f32[64,64,64]{0,2,1:T(8,128)} %copy-done.2) | data formatting | bytes 2097152
  106.9 3.8 %copy.78 = f32[64,64,64]{2,1,0:T(8,128)} copy(f32[64,64,64]{0,2,1:T(8,128)} %copy-done.1) | data formatting | bytes 2097152
  111.0 0.3 convolution_bitcast_fusion
  111.3 0.3 fusion.44
  111.7 3.3 %all-reduce = (f32[64,20]{0,1:T(8,128)S(1)}, f32[64]{0:T(128)S(1)}) all-reduce(f32[64,20]{0,1:T(8,128)S(1)} %fusion.44, f32[64]{0:T(128)S(1)} %convolution_bitcast_fusion), channel_id=1, replica_groups=mesh['ep'=16,'tp'=2] {'tp'}, use_global_device_ids=true, to_apply=%region_5.0 | all-reduce | flops 1344 | bytes 10752 | tf_op jit(solution)/shard_map/psum | solution.py:127
  115.1 3.4 %all-gather.2.cloned.1.call-done = bf16[1024,1024]{1,0:T(8,128)(2,1)} async-done(((bf16[64,1024]{1,0:T(8,128)(2,1)}), bf16[1024,1024]{1,0:T(8,128)(2,1)}) %all-gather.2.cloned.1.call-update) | async-done | bytes 2097168 | tf_op jit(solution)/shard_map/all_gather | solution.py:170
  118.5 2.4 %convolution_convert_fusion.4 = bf16[1024,128]{0,1:T(8,128)(2,1)S(1)} fusion(bf16[1024,1024]{1,0:T(8,128)(2,1)} %all-gather.2.cloned.1.call-done, bf16[1024,128]{1,0:T(8,128)(2,1)S(1)} %copy-done.12), kind=kOutput, calls=%fused_computation.17 | convolution fusion | flops 268566528 | bytes 2621440 | tf_op jit(solution)/shard_map/dot_general | solution.py:54
  120.9 7.1 %reduce-scatter.5.cloned.1.call-done = bf16[256,1024]{1,0:T(8,128)(2,1)} async-done(((bf16[256,2048]{1,0:T(8,128)(2,1)}), bf16[256,1024]{1,0:T(8,128)(2,1)}) %reduce-scatter.5.cloned.1.call-update) | async-done | bytes 524304 | tf_op jit(solution)/shard_map/reduce_scatter | solution.py:163
  128.0 6.8 %all-to-all-start.1 = ((bf16[16,16,1024]{2,1,0:T(8,128)(2,1)}), bf16[16,16,1024]{2,1,0:T(8,128)(2,1)S(1)}, u32[]{:S(2)}, u32[]{:S(2)}) async-start(bf16[16,16,1024]{2,1,0:T(8,128)(2,1)} %bitcast.80), calls=%async_computation.3 | async-start | bytes 1048576 | tf_op jit(solution)/shard_map/all_to_all | solution.py:165
  134.9 2.4 %convolution_convert_fusion.5 = bf16[1024,128]{0,1:T(8,128)(2,1)S(1)} fusion(bf16[1024,1024]{1,0:T(8,128)(2,1)} %all-gather.2.cloned.1.call-done, bf16[1024,128]{1,0:T(8,128)(2,1)S(1)} %copy-done.13), kind=kOutput, calls=%fused_computation.18 | convolution fusion | flops 268566528 | bytes 2621440 | tf_op jit(solution)/shard_map/dot_general | solution.py:53
  137.3 0.8 pad_maximum_fusion.1
  138.2 20.0 %all-reduce.3.cloned.1.call-done = bf16[1024,256]{0,1:T(8,128)(2,1)} async-done(((bf16[1024,256]{0,1:T(8,128)(2,1)}), bf16[1024,256]{0,1:T(8,128)(2,1)}) %all-reduce.3.cloned.1.call-update) | async-done | bytes 524304 | tf_op jit(solution)/shard_map/psum | solution.py:172
  158.2 1.1 convert_element_type.84
  159.4 0.2 fusion.17
  159.5 0.8 copy.75
  160.3 6.8 %all-to-all-start.2 = ((bf16[16,64,128]{2,1,0:T(8,128)(2,1)}), bf16[16,64,128]{2,1,0:T(8,128)(2,1)S(1)}, u32[]{:S(2)}, u32[]{:S(2)}) async-start(bf16[16,64,128]{2,1,0:T(8,128)(2,1)} %bitcast.19), calls=%async_computation.4 | async-start | bytes 524288 | tf_op jit(solution)/shard_map/all_to_all | solution.py:177
  167.3 0.9 gather_fusion
  168.2 0.3 reshape.153
  168.5 0.7 multiply_reduce_fusion
  169.2 8.2 %all-to-all-done.2 = bf16[16,64,128]{2,1,0:T(8,128)(2,1)S(1)} async-done(((bf16[16,64,128]{2,1,0:T(8,128)(2,1)}), bf16[16,64,128]{2,1,0:T(8,128)(2,1)S(1)}, u32[]{:S(2)}, u32[]{:S(2)}) %all-to-all-start.2) | async-done | bytes 262176 | tf_op jit(solution)/shard_map/all_to_all | solution.py:177
  177.5 3.7 %fusion.14 = bf16[64,1024]{1,0:T(8,128)(2,1)} fusion(bf16[2048,1024]{1,0:T(8,128)(2,1)} %param.49, f32[64,1024]{1,0:T(8,128)S(1)} %multiply_reduce_fusion, bf16[64,1024]{1,0:T(8,128)(2,1)S(1)} %get-tuple-element.15, f32[64]{0:T(128)S(1)} %add_divide_fusion, bf16[16,64,128]{2,1,0:T(8,128)(2,1)S(1)} %all-to-all-done.2), kind=kOutput, calls=%fused_computation.21 | convolution fusion | flops 268763136 | bytes 4980992 | tf_op jit(solution)/shard_map/dot_general | solution.py:178
  (85 shorter events, 1.7 us)
Async XLA Ops:
  7.2 91.7 %copy-start = (bf16[1,512,2048]{2,1,0:T(8,128)(2,1)S(1)}, bf16[1,512,2048]{2,1,0:T(8,128)(2,1)}, u32[]{:S(2)}) copy-start(bf16[1,512,2048]{2,1,0:T(8,128)(2,1)} %param.46) | copy-start | bytes 6291460
  7.2 40.9 %reduce-scatter.3.cloned.1.call-start = ((), (), s32[]{:S(2)}) async-start(), calls=%async_computation.5 | async-start | bytes 786432 | tf_op jit(solution)/shard_map/reduce_scatter | solution.py:110
  10.7 3.4 %copy-start.6 = (bf16[64,1024]{1,0:T(8,128)(2,1)S(1)}, bf16[64,1024]{1,0:T(8,128)(2,1)}, u32[]{:S(2)}) copy-start(bf16[64,1024]{1,0:T(8,128)(2,1)} %param.25) | copy-start | bytes 393220
  10.7 6.2 %copy-start.18 = (f32[2048]{0:T(1024)S(1)}, f32[2048]{0:T(1024)}, u32[]{:S(2)}) copy-start(f32[2048]{0:T(1024)} %param.28) | copy-start | bytes 24580
  10.7 8.0 %copy-start.21 = (f32[64]{0:T(128)S(1)}, f32[64]{0:T(128)}, u32[]{:S(2)}) copy-start(f32[64]{0:T(128)} %param.32) | copy-start | bytes 772
  10.7 9.1 %copy-start.7 = (f32[64,64,16]{1,2,0:T(8,128)S(1)}, f32[64,64,16]{1,2,0:T(8,128)}, u32[]{:S(2)}) copy-start(f32[64,64,16]{1,2,0:T(8,128)} %param.34) | copy-start | bytes 786436
  10.7 9.1 %copy-start.8 = (f32[64,64,16]{1,2,0:T(8,128)S(1)}, f32[64,64,16]{1,2,0:T(8,128)}, u32[]{:S(2)}) copy-start(f32[64,64,16]{1,2,0:T(8,128)} %param.33) | copy-start | bytes 786436
  19.8 5.0 %copy-start.3 = (f32[64,64,64]{0,2,1:T(8,128)S(1)}, f32[64,64,64]{0,2,1:T(8,128)}, u32[]{:S(2)}) copy-start(f32[64,64,64]{0,2,1:T(8,128)} %copy.64) | copy-start | bytes 3145732
  19.8 5.0 %copy-start.4 = (f32[64,64,64]{0,2,1:T(8,128)S(1)}, f32[64,64,64]{0,2,1:T(8,128)}, u32[]{:S(2)}) copy-start(f32[64,64,64]{0,2,1:T(8,128)} %copy.63) | copy-start | bytes 3145732
  24.8 3.3 %copy-start.2 = (f32[64,64,64]{0,2,1:T(8,128)}, f32[64,64,64]{0,2,1:T(8,128)S(1)}, u32[]{:S(2)}) copy-start(f32[64,64,64]{0,2,1:T(8,128)S(1)} %bitcast_add_fusion.1) | copy-start | bytes 3145732
  24.8 3.3 %copy-start.11 = (f32[64,16,64]{2,1,0:T(8,128)S(1)}, f32[64,16,64]{2,1,0:T(8,128)}, u32[]{:S(2)}) copy-start(f32[64,16,64]{2,1,0:T(8,128)} %param.35) | copy-start | bytes 786436
  28.0 3.9 %copy-start.1 = (f32[64,64,64]{0,2,1:T(8,128)}, f32[64,64,64]{0,2,1:T(8,128)S(1)}, u32[]{:S(2)}) copy-start(f32[64,64,64]{0,2,1:T(8,128)S(1)} %bitcast_add_fusion) | copy-start | bytes 3145732
  28.0 1.9 %copy-start.10 = (f32[64,16,64]{2,1,0:T(8,128)S(1)}, f32[64,16,64]{2,1,0:T(8,128)}, u32[]{:S(2)}) copy-start(f32[64,16,64]{2,1,0:T(8,128)} %param.36) | copy-start | bytes 786436
  30.0 2.1 %copy-start.14 = (f32[1024]{0:T(1024)S(1)}, f32[1024]{0:T(1024)}, u32[]{:S(2)}) copy-start(f32[1024]{0:T(1024)} %param.37) | copy-start | bytes 12292
  32.1 3.5 %copy-start.5 = (bf16[1024,2048]{1,0:T(8,128)(2,1)S(1)}, bf16[1024,2048]{1,0:T(8,128)(2,1)}, u32[]{:S(2)}) copy-start(bf16[1024,2048]{1,0:T(8,128)(2,1)} %param.38) | copy-start | bytes 12582916
  35.6 1.9 %copy-start.19 = (f32[2048]{0:T(1024)S(1)}, f32[2048]{0:T(1024)}, u32[]{:S(2)}) copy-start(f32[2048]{0:T(1024)} %param.29) | copy-start | bytes 24580
  35.6 1.9 %copy-start.16 = (s32[64,2]{0,1:T(2,128)S(1)}, s32[64,2]{0,1:T(2,128)}, u32[]{:S(2)}) copy-start(s32[64,2]{0,1:T(2,128)} %param.43) | copy-start | bytes 1540
  37.4 81.1 %all-gather.2.cloned.1.call-start = ((), (), s32[]{:S(2)}) async-start(), calls=%async_computation.7 | async-start | bytes 2228224 | tf_op jit(solution)/shard_map/all_gather | solution.py:170
  52.5 75.5 %reduce-scatter.5.cloned.1.call-start = ((), (), s32[]{:S(2)}) async-start(), calls=%async_computation.6 | async-start | bytes 1572864 | tf_op jit(solution)/shard_map/reduce_scatter | solution.py:163
  53.3 44.9 %copy-start.20 = (bf16[1,2048,512]{2,1,0:T(8,128)(2,1)S(1)}, bf16[1,2048,512]{2,1,0:T(8,128)(2,1)}, u32[]{:S(2)}) copy-start(bf16[1,2048,512]{2,1,0:T(8,128)(2,1)} %param.44) | copy-start | bytes 6291460
  97.2 1.0 copy-start.9
  106.9 4.0 %copy-start.17 = (bf16[2048,4]{0,1:T(4,128)(2,1)S(1)}, bf16[2048,4]{0,1:T(4,128)(2,1)}, u32[]{:S(2)}) copy-start(bf16[2048,4]{0,1:T(4,128)(2,1)} %param.40) | copy-start | bytes 49156
  106.9 4.0 %copy-start.15 = (bf16[2048,16]{0,1:T(8,128)(2,1)S(1)}, bf16[2048,16]{0,1:T(8,128)(2,1)}, u32[]{:S(2)}) copy-start(bf16[2048,16]{0,1:T(8,128)(2,1)} %param.41) | copy-start | bytes 196612
  106.9 4.1 %dynamic-slice-start = ((f32[2048]{0:T(1024)}, s32[]{:T(128)}), f32[1024]{0:T(1024)S(1)}, s32[]{:S(2)}) async-start(f32[2048]{0:T(1024)} %param.42, s32[]{:T(128)} %select_n.30), calls=%async_computation.9 | async-start | bytes 8704 | tf_op jit(solution)/shard_map/dynamic_slice | solution.py:90
  106.9 11.6 %copy-start.12 = (bf16[1024,128]{1,0:T(8,128)(2,1)S(1)}, bf16[1024,128]{1,0:T(8,128)(2,1)}, u32[]{:S(2)}) copy-start(bf16[1024,128]{1,0:T(8,128)(2,1)} %param.48) | copy-start | bytes 786436
  111.0 23.9 %copy-start.13 = (bf16[1024,128]{1,0:T(8,128)(2,1)S(1)}, bf16[1024,128]{1,0:T(8,128)(2,1)}, u32[]{:S(2)}) copy-start(bf16[1024,128]{1,0:T(8,128)(2,1)} %param.47) | copy-start | bytes 786436
  128.0 32.3 %all-to-all-start.1 = ((bf16[16,16,1024]{2,1,0:T(8,128)(2,1)}), bf16[16,16,1024]{2,1,0:T(8,128)(2,1)S(1)}, u32[]{:S(2)}, u32[]{:S(2)}) async-start(bf16[16,16,1024]{2,1,0:T(8,128)(2,1)} %bitcast.80), calls=%async_computation.3 | async-start | bytes 1048576 | tf_op jit(solution)/shard_map/all_to_all | solution.py:165
  134.8 23.4 %all-reduce.3.cloned.1.call-start = ((), (), s32[]{:S(2)}) async-start(), calls=%async_computation.8 | async-start | bytes 1048576 | tf_op jit(solution)/shard_map/psum | solution.py:172
  160.3 17.1 %all-to-all-start.2 = ((bf16[16,64,128]{2,1,0:T(8,128)(2,1)}), bf16[16,64,128]{2,1,0:T(8,128)(2,1)S(1)}, u32[]{:S(2)}, u32[]{:S(2)}) async-start(bf16[16,64,128]{2,1,0:T(8,128)(2,1)} %bitcast.19), calls=%async_computation.4 | async-start | bytes 524288 | tf_op jit(solution)/shard_map/all_to_all | solution.py:177
Sparse Core Ops, SparseCore 0:
  37.6 10.4 reduce-scatter.2
  52.6 65.8 all-gather.1
  120.8 7.2 reduce-scatter.4
  138.3 19.8 all-reduce.2
where the time goes:
time: 188 us
  blocking collectives  51.7 us (28%)
  waiting for transfers between devices  49.1 us (26%)
  matrix products  30.9 us (16%)
  local copies, waits for them, and re-layouts  19.7 us (10%)
  between operations  14.3 us (8%)
  starting transfers between devices  13.8 us (7%)
  other arithmetic  8.23 us (4%)
    all_to_all x1, blocking collectives, shards(): lax.all_to_all(outgoing, 'ep', split_axis=0, concat_axis=0, tiled=True)  41 us
    psum x1, waiting for transfers between devices, shards(): lax.psum(partial_dense.astype(jnp.bfloat16), 'tp').astype(jnp.float32)  20 us
    unnamed x49, local copies, waits for them, and re-layouts  15.8 us
    reduce_scatter x1, waiting for transfers between devices, shards(): lax.psum_scatter(stacked.astype(jnp.bfloat16), 'tp', scatter_dimension=2,...  10.3 us
    all_to_all x1, waiting for transfers between devices, shards(): lax.all_to_all(inner_cols, 'ep', split_axis=0, concat_axis=1, tiled=True)  8.24 us
    reduce_scatter x1, waiting for transfers between devices, shards(): lax.psum_scatter(part_out.astype(jnp.bfloat16), 'tp', scatter_dimension=1...  7.08 us
    all_to_all x1, starting transfers between devices, shards(): lax.all_to_all(inner_cols, 'ep', split_axis=0, concat_axis=1, tiled=True)  6.83 us
    all_to_all x1, starting transfers between devices, shards(): lax.all_to_all(finished, 'ep', split_axis=0, concat_axis=0, tiled=True)  6.79 us
  transfers between devices with their start and end apart: 6, of which 5 were waited for; matrix products, arithmetic and copies ran while one was open for 13% of the time, Pallas kernels for 0%

commit v1 on v0

v1 whole, which is shorter than its diff:
```python
import functools

import jax
import jax.numpy as jnp
from jax import lax
from jax.experimental import pallas as pl
from jax.experimental.pallas import tpu as pltpu
from jax.sharding import PartitionSpec as P

NG = 4
LANES = 128
MESH = pl.DeviceIdType.MESH
VMEM = pl.BlockSpec(memory_space=pltpu.VMEM)


EPS = 1e-06


def state_factors(rate, freq, log_group_step, input_map_real, input_map_imaginary):
    step_size = jnp.exp(log_group_step)[:, None]
    magnitude = jnp.exp(-rate * step_size)
    abar_re = magnitude * jnp.cos(freq * step_size)
    abar_im = magnitude * jnp.sin(freq * step_size)
    denom = rate * rate + freq * freq
    shift_re = abar_re - 1.0
    fac_re = (abar_im * freq - shift_re * rate) / denom
    fac_im = -(abar_im * rate + shift_re * freq) / denom
    bbar_re = fac_re[:, :, None] * input_map_real - fac_im[:, :, None] * input_map_imaginary
    bbar_im = fac_re[:, :, None] * input_map_imaginary + fac_im[:, :, None] * input_map_real
    return (abar_re, abar_im, bbar_re, bbar_im)


def ep_dims(count):
    bits = count.bit_length() - 1
    if 1 << bits != count:
        return (count, 1, 1)
    return (1 << ((bits + 2) // 3), 1 << ((bits + 1) // 3), 1 << (bits // 3))


def mixer_kernel(
    channels, normed_ref, re_ref, im_ref, ar_ref, ai_ref, br_ref, bi_ref, cr_ref, ci_ref, skip_ref,
    act_ref, nre_ref, nim_ref,
):
    rows, lanes = normed_ref.shape
    groups, states = re_ref.shape[1:]
    u = normed_ref[...].astype(jnp.float32)
    lane = lax.broadcasted_iota(jnp.int32, (groups, lanes), 1)
    group = lax.broadcasted_iota(jnp.int32, (groups, lanes), 0)
    mask = jnp.where((lane >= group * channels) & (lane < group * channels + channels), 1.0, 0.0)
    spread = (u[:, None, :] * mask[None]).reshape(rows * groups, lanes).astype(jnp.bfloat16)
    drive_re = jnp.dot(spread, br_ref[...], preferred_element_type=jnp.float32)
    drive_im = jnp.dot(spread, bi_ref[...], preferred_element_type=jnp.float32)
    a_re, a_im = ar_ref[...][None], ai_ref[...][None]
    s_re, s_im = re_ref[...], im_ref[...]
    n_re = a_re * s_re - a_im * s_im + drive_re.reshape(rows, groups, states)
    n_im = a_re * s_im + a_im * s_re + drive_im.reshape(rows, groups, states)
    nre_ref[...] = n_re
    nim_ref[...] = n_im
    dims = (((1,), (1,)), ((), ()))
    flat_re = n_re.reshape(rows * groups, states).astype(jnp.bfloat16)
    flat_im = n_im.reshape(rows * groups, states).astype(jnp.bfloat16)
    read = lax.dot_general(flat_re, cr_ref[...], dims, preferred_element_type=jnp.float32)
    read = read - lax.dot_general(flat_im, ci_ref[...], dims, preferred_element_type=jnp.float32)
    mixed = jnp.sum(read.reshape(rows, groups, lanes) * mask[None], axis=1) + skip_ref[...] * u
    act_ref[...] = jax.nn.gelu(mixed).astype(jnp.bfloat16)


def mixer(normed, state_re, state_im, factors, out_re, out_im, skip):
    abar_re, abar_im, bbar_re, bbar_im = factors
    rows, width = normed.shape
    groups, states = abar_re.shape
    channels = width // groups
    per = LANES // channels
    maps = [
        jnp.swapaxes(b, 1, 2).reshape(width, states).astype(jnp.bfloat16) for b in (bbar_re, bbar_im)
    ] + [o.reshape(width, states).astype(jnp.bfloat16) for o in (out_re, out_im)]
    cols = pl.BlockSpec((rows, LANES), lambda i: (0, i))
    state = pl.BlockSpec((rows, per, states), lambda i: (0, i, 0))
    abar = pl.BlockSpec((per, states), lambda i: (i, 0))
    chan = pl.BlockSpec((LANES, states), lambda i: (i, 0))
    return pl.pallas_call(
        functools.partial(mixer_kernel, channels),
        grid=(width // LANES,),
        in_specs=[cols, state, state, abar, abar, chan, chan, chan, chan,
                  pl.BlockSpec((1, LANES), lambda i: (0, i))],
        out_specs=[cols, state, state],
        out_shape=[
            jax.ShapeDtypeStruct((rows, width), jnp.bfloat16),
            jax.ShapeDtypeStruct(state_re.shape, jnp.float32),
            jax.ShapeDtypeStruct(state_re.shape, jnp.float32),
        ],
        name="mixer",
    )(normed, state_re, state_im, abar_re, abar_im, *maps, skip[None, :])


def greet(peers):
    barrier = pltpu.get_barrier_semaphore()
    for peer in peers:
        pl.semaphore_signal(barrier, inc=1, device_id=peer, device_id_type=MESH)
    pl.semaphore_wait(barrier, len(peers))


def remote(src, dst, send, recv, peer):
    return pltpu.make_async_remote_copy(
        src_ref=src, dst_ref=dst, send_sem=send, recv_sem=recv, device_id=peer, device_id_type=MESH
    )


def pair_kernel(count, *refs):
    sources, targets, (send, recv) = refs[:count], refs[count:2 * count], refs[2 * count:]
    peer = (lax.axis_index("ep"), 1 - lax.axis_index("tp"))
    greet([peer])
    copies = [remote(s, t, send.at[i], recv.at[i], peer) for i, (s, t) in enumerate(zip(sources, targets))]
    for copy in copies:
        copy.start()
    for copy in copies:
        copy.wait()


def pair_swap(number, *arrays):
    count = len(arrays)
    return pl.pallas_call(
        functools.partial(pair_kernel, count),
        in_specs=[VMEM] * count,
        out_specs=[VMEM] * count,
        out_shape=[jax.ShapeDtypeStruct(a.shape, a.dtype) for a in arrays],
        scratch_shapes=[pltpu.SemaphoreType.DMA((count,))] * 2,
        compiler_params=pltpu.CompilerParams(collective_id=number, has_side_effects=True),
        name="pair_swap",
    )(*arrays)


def gather_plan(units):
    first = units // 8
    second = (units - first + 1) // 2
    return [(0, first, (2, 1, 0)), (first, second, (0, 1, 2)), (first + second, units - first - second, (0, 2, 1))]


def hidden_kernel(
    dims, width, keep_ref, send_ref, tokens_ref, gain_ref, router_ref, ranks_ref,
    hidden_ref, stats_ref, rows_ref, rank_out_ref,
    vg_buf, stat_buf, stat_in, pair_send, pair_recv, send, recv,
):
    ep, tp = lax.axis_index("ep"), lax.axis_index("tp")
    me = (ep // (dims[1] * dims[2]), (ep // dims[2]) % dims[1], ep % dims[2])
    partner = (ep, 1 - tp)

    def neighbour(dim, step):
        c = [me[d] if d != dim else lax.rem(me[d] + step, dims[d]) for d in range(3)]
        return ((c[0] * dims[1] + c[1]) * dims[2] + c[2], tp)

    greet([partner] + [neighbour(d, s) for d in range(3) for s in range(1, dims[d])])
    swap = remote(send_ref, vg_buf, pair_send.at[0], pair_recv.at[0], partner)
    swap.start()
    rank_out_ref[me[0], me[1], me[2]] = ranks_ref[...]
    swap.wait()
    rows, half = tokens_ref.shape
    value = keep_ref[0].astype(jnp.float32) + vg_buf[0].astype(jnp.float32)
    gate = keep_ref[1].astype(jnp.float32) + vg_buf[1].astype(jnp.float32)
    mix = (value * jax.nn.sigmoid(gate)).astype(jnp.bfloat16).astype(jnp.float32)
    hidden = (tokens_ref[...].astype(jnp.float32) + mix).astype(jnp.bfloat16)
    hidden_ref[...] = hidden
    hidden = hidden.astype(jnp.float32)
    scaled = hidden * gain_ref[...]
    raw = jnp.dot(scaled.astype(jnp.bfloat16), router_ref[...], preferred_element_type=jnp.float32)
    squares = jnp.sum(hidden * hidden, axis=1, keepdims=True)
    lane = lax.broadcasted_iota(jnp.int32, raw.shape, 1)
    stat_buf[...] = jnp.where(lane == LANES - 1, squares, raw)
    swap = remote(stat_buf, stat_in, pair_send.at[1], pair_recv.at[1], partner)
    swap.start()
    swap.wait()
    total = stat_buf[...] + stat_in[...]
    inverse = lax.rsqrt(total[:, LANES - 1:] / width + EPS)
    stats_ref[...] = total * inverse
    rows_ref[me[0], me[1], me[2]] = (scaled * inverse).astype(jnp.bfloat16)

    paths = [(rows_ref, lo * LANES, n * LANES, order) for lo, n, order in gather_plan(half // LANES) if n]
    paths = [(rank_out_ref, 0, LANES, (2, 1, 0))] + paths
    slots = sum(d - 1 for d in dims)
    pending = [[] for _ in paths]
    for stage in range(3):
        for p, (ref, lo, n, order) in enumerate(paths):
            for copy in pending[p]:
                copy.wait_recv()
            dim = order[stage]
            done = order[:stage]
            where = tuple(pl.ds(0, dims[d]) if d in done else pl.ds(me[d], 1) for d in range(3))
            block = ref.at[where + (pl.ds(0, rows), pl.ds(lo, n))]
            base = p * slots + sum(dims[d] - 1 for d in done)
            fresh = [
                remote(block, block, send.at[base + s - 1], recv.at[base + s - 1], neighbour(dim, s))
                for s in range(1, dims[dim])
            ]
            for copy in fresh:
                copy.start()
            for copy in pending[p]:
                copy.wait_send()
            pending[p] = fresh
    for copies in pending:
        for copy in copies:
            copy.wait()


def hidden_rows(dims, width, keep, give, tokens, gain, router, ranks):
    rows, half = tokens.shape
    slots = 4 * sum(d - 1 for d in dims)
    return pl.pallas_call(
        functools.partial(hidden_kernel, dims, width),
        in_specs=[VMEM] * 6,
        out_specs=[VMEM] * 4,
        out_shape=[
            jax.ShapeDtypeStruct((rows, half), jnp.bfloat16),
            jax.ShapeDtypeStruct((rows, LANES), jnp.float32),
            jax.ShapeDtypeStruct(dims + (rows, half), jnp.bfloat16),
            jax.ShapeDtypeStruct(dims + (rows, LANES), jnp.bfloat16),
        ],
        scratch_shapes=[
            pltpu.VMEM((2, rows, half), jnp.bfloat16),
            pltpu.VMEM((rows, LANES), jnp.float32),
            pltpu.VMEM((rows, LANES), jnp.float32),
            pltpu.SemaphoreType.DMA((2,)),
            pltpu.SemaphoreType.DMA((2,)),
            pltpu.SemaphoreType.DMA((slots,)),
            pltpu.SemaphoreType.DMA((slots,)),
        ],
        compiler_params=pltpu.CompilerParams(collective_id=2, has_side_effects=True),
        name="hidden_rows",
    )(keep, give, tokens, gain, router, ranks)


def return_kernel(
    n, keep_ref, give_ref, dense_ref, ret_ref, dense_out_ref,
    got, summed, pair_send, pair_recv, e_send, e_recv, d_send, d_recv, local,
):
    ep, tp = lax.axis_index("ep"), lax.axis_index("tp")
    partner = (ep, 1 - tp)
    peers = [lax.rem(ep + s, n) for s in range(1, n)]
    greet([partner] + [(q, tp) for q in peers])
    swap = remote(give_ref, got, pair_send.at[0], pair_recv.at[0], partner)
    swap.start()
    dense_own = pltpu.make_async_copy(dense_ref.at[ep], dense_out_ref.at[tp, ep], local.at[0])
    dense_own.start()
    dense = [
        remote(dense_ref.at[q], dense_out_ref.at[tp, ep], d_send.at[i], d_recv.at[i], (q, tp))
        for i, q in enumerate(peers)
    ]
    for copy in dense:
        copy.start()
    swap.wait()
    summed[...] = (keep_ref[...].astype(jnp.float32) + got[...].astype(jnp.float32)).astype(jnp.bfloat16)
    own = pltpu.make_async_copy(summed.at[ep], ret_ref.at[ep], local.at[1])
    own.start()
    experts = [
        remote(summed.at[q], ret_ref.at[ep], e_send.at[i], e_recv.at[i], (q, tp))
        for i, q in enumerate(peers)
    ]
    for copy in experts:
        copy.start()
    dense_own.wait()
    for copy in dense:
        copy.wait_recv()
    share = remote(
        dense_out_ref.at[tp], dense_out_ref.at[tp], pair_send.at[1], pair_recv.at[1], partner
    )
    share.start()
    for copy in dense:
        copy.wait_send()
    own.wait()
    for copy in experts:
        copy.wait()
    share.wait()


def return_rows(keep, give, dense):
    n = keep.shape[0]
    dma = pltpu.SemaphoreType.DMA
    return pl.pallas_call(
        functools.partial(return_kernel, n),
        in_specs=[VMEM] * 3,
        out_specs=[VMEM] * 2,
        out_shape=[
            jax.ShapeDtypeStruct(keep.shape, jnp.bfloat16),
            jax.ShapeDtypeStruct((2,) + dense.shape, jnp.bfloat16),
        ],
        scratch_shapes=[
            pltpu.VMEM(keep.shape, jnp.bfloat16),
            pltpu.VMEM(keep.shape, jnp.bfloat16),
            dma((2,)), dma((2,)),
            dma((n - 1,)), dma((n - 1,)), dma((n - 1,)), dma((n - 1,)), dma((2,)),
        ],
        compiler_params=pltpu.CompilerParams(collective_id=3, has_side_effects=True),
        name="return_rows",
    )(keep, give, dense)


def shards(
    ep_count,
    tokens,
    sequence_state_real,
    sequence_state_imaginary,
    mixer_norm_gain,
    expert_norm_gain,
    rate,
    freq,
    log_group_step,
    input_map_real,
    input_map_imaginary,
    output_map_real,
    output_map_imaginary,
    skip,
    mixer_value_weight,
    mixer_gate_weight,
    group_router_weight,
    expert_router_weight,
    dense_blend_weight,
    routes,
    expert_gate_weight,
    expert_up_weight,
    expert_down_weight,
    shared_gate_weight,
    shared_up_weight,
    shared_down_weight,
):
    seq_rows, half_width = tokens.shape
    width = 2 * half_width
    ep, tp = lax.axis_index("ep"), lax.axis_index("tp")
    column_start = tp * half_width

    def own_rows(values):
        return lax.dynamic_slice_in_dim(values, column_start, half_width, 0)

    def own_cols(values, core):
        return lax.dynamic_slice_in_dim(values, core * half_width, half_width, values.ndim - 1)

    experts = expert_router_weight.shape[1]
    top_count = routes.shape[1]
    per_group = experts // NG
    capacity = max(2, 2 * seq_rows * top_count // experts)
    hits = routes[:, :, None] == jnp.arange(experts, dtype=jnp.int32)[None, None, :]
    named = jnp.any(hits, axis=1)
    order = jnp.arange(seq_rows)
    earlier = (order[None, :] <= order[:, None]).astype(jnp.bfloat16)
    counted = jnp.dot(earlier, named.astype(jnp.bfloat16), preferred_element_type=jnp.float32)
    ranks_f32 = jnp.where(named, counted, 0.0)
    ranks = jnp.pad(ranks_f32.astype(jnp.bfloat16), ((0, 0), (0, LANES - experts)))

    float_tokens = tokens.astype(jnp.float32)
    square_sum = lax.psum(jnp.sum(float_tokens * float_tokens, axis=1), "tp")
    first_scale = lax.rsqrt(square_sum / width + EPS)[:, None]
    normed = (float_tokens * first_scale * own_rows(mixer_norm_gain)).astype(jnp.bfloat16)
    factors = state_factors(rate, freq, log_group_step, input_map_real, input_map_imaginary)
    activated, next_re, next_im = mixer(
        normed, sequence_state_real, sequence_state_imaginary, factors,
        output_map_real, output_map_imaginary, skip,
    )
    value_part = jnp.dot(activated, mixer_value_weight, preferred_element_type=jnp.float32)
    gate_part = jnp.dot(activated, mixer_gate_weight, preferred_element_type=jnp.float32)
    stacked = jnp.stack([value_part.astype(jnp.bfloat16), gate_part.astype(jnp.bfloat16)], axis=0)
    router_map = jnp.concatenate(
        [
            own_rows(group_router_weight),
            own_rows(expert_router_weight),
            own_rows(dense_blend_weight).astype(jnp.bfloat16)[:, None],
        ],
        axis=1,
    )
    router_map = jnp.pad(router_map, ((0, 0), (0, LANES - router_map.shape[1])))
    hidden, stats, gathered, gathered_ranks = hidden_rows(
        ep_dims(ep_count), width, own_cols(stacked, tp), own_cols(stacked, 1 - tp), tokens,
        own_rows(expert_norm_gain)[None, :], router_map, ranks,
    )
    rows = gathered.reshape(ep_count * seq_rows, half_width)
    rank_rows = gathered_ranks.reshape(ep_count * seq_rows, LANES)
    lane = jnp.arange(LANES, dtype=jnp.int32)[None, :]
    mine = jnp.sum(jnp.where(lane == ep, rank_rows.astype(jnp.float32), 0.0), axis=1).astype(jnp.int32)
    source = jnp.arange(ep_count * seq_rows, dtype=jnp.int32) // seq_rows
    slot = jnp.where(mine > 0, source * capacity + mine - 1, -1)
    dispatch = slot[None, :] == jnp.arange(ep_count * capacity, dtype=jnp.int32)[:, None]
    half_rows = jnp.dot(
        dispatch.astype(jnp.bfloat16), rows, preferred_element_type=jnp.float32
    ).astype(jnp.bfloat16)

    half_seq = seq_rows // 2
    dense_cols = shared_gate_weight.shape[1]
    dense_part = jnp.stack(
        [
            jnp.dot(rows, w, preferred_element_type=jnp.float32).astype(jnp.bfloat16)
            for w in (shared_gate_weight, shared_up_weight)
        ]
    ).reshape(2, ep_count, 2, half_seq, dense_cols)

    def token_half(core):
        return lax.dynamic_index_in_dim(dense_part, core, 2, keepdims=False)

    other_rows, dense_got = pair_swap(1, half_rows, token_half(1 - tp))
    dense_sum = token_half(tp).astype(jnp.float32) + dense_got.astype(jnp.float32)
    dense_inner = (jax.nn.silu(dense_sum[0]) * dense_sum[1]).astype(jnp.bfloat16)

    first_rows = jnp.where(tp == 0, half_rows, other_rows)
    second_rows = jnp.where(tp == 0, other_rows, half_rows)
    token_rows = jnp.concatenate([first_rows, second_rows], axis=1)
    gate_e = jnp.dot(token_rows, expert_gate_weight[0], preferred_element_type=jnp.float32)
    up_e = jnp.dot(token_rows, expert_up_weight[0], preferred_element_type=jnp.float32)
    inner = (jax.nn.silu(gate_e) * up_e).astype(jnp.bfloat16)
    part_out = jnp.dot(inner, expert_down_weight[0], preferred_element_type=jnp.float32).astype(jnp.bfloat16)
    part_out = part_out.reshape(ep_count, capacity, width)
    returned, dense_all = return_rows(own_cols(part_out, tp), own_cols(part_out, 1 - tp), dense_inner)

    logits, blend_logit = stats[:, :NG + experts], stats[:, NG + experts]
    group_prob = jax.nn.softmax(logits[:, :NG], axis=-1)
    chosen = jnp.sum(jnp.where(hits, logits[:, None, NG:], 0.0), axis=2)
    group_hits = (routes // per_group)[:, :, None] == jnp.arange(NG, dtype=jnp.int32)[None, None, :]
    group_sel = jnp.sum(jnp.where(group_hits, group_prob[:, None, :], 0.0), axis=2)
    weights = jax.nn.softmax(chosen, axis=1) * group_sel
    expert_weight = jnp.sum(jnp.where(hits, weights[:, :, None], 0.0), axis=1)
    places = jnp.arange(capacity, dtype=jnp.float32) + 1.0
    combine = jnp.where(ranks_f32[:, :, None] == places[None, None, :], expert_weight[:, :, None], 0.0)
    combine = combine.reshape(seq_rows, experts * capacity).astype(jnp.bfloat16)
    routed = jnp.dot(
        combine, returned.reshape(experts * capacity, half_width), preferred_element_type=jnp.float32
    )
    dense_rows = jnp.transpose(dense_all, (0, 2, 1, 3)).reshape(seq_rows, ep_count * dense_cols)
    dense_out = jnp.dot(dense_rows, shared_down_weight, preferred_element_type=jnp.float32)
    result = hidden.astype(jnp.float32) + routed + jax.nn.sigmoid(blend_logit)[:, None] * dense_out
    return (result.astype(jnp.bfloat16), next_re, next_im)


def solution(mesh):
    placed = (
        P("ep", "tp"),
        P("ep", "tp", None),
        P("ep", "tp", None),
        P(),
        P(),
        P("tp", None),
        P("tp", None),
        P("tp"),
        P("tp", None, None),
        P("tp", None, None),
        P("tp", None, None),
        P("tp", None, None),
        P("tp"),
        P("tp", None),
        P("tp", None),
        P(),
        P(),
        P(),
        P("ep", None),
        P("ep", None, "tp"),
        P("ep", None, "tp"),
        P("ep", "tp", None),
        P("tp", "ep"),
        P("tp", "ep"),
        P(None, "tp"),
    )
    return jax.shard_map(
        functools.partial(shards, mesh.shape["ep"]),
        mesh=mesh,
        in_specs=placed,
        out_specs=(P("ep", "tp"), P("ep", "tp", None), P("ep", "tp", None)),
        check_vma=False,
    )
```

time: 188 us -> 124 us (0.66); the launches traced: 188 us -> 122 us
  Pallas kernels: 0 us -> 69.6 us
  waiting for transfers between devices: 49.1 us -> 0 us
  blocking collectives: 51.7 us -> 2.63 us
  starting transfers between devices: 13.8 us -> 0 us
  between operations: 14.3 us -> 0.94 us
  matrix products: 30.9 us -> 18.7 us
  other arithmetic: 8.23 us -> 18.8 us
  local copies, waits for them, and re-layouts: 19.7 us -> 11.2 us
    pallas_call x0 -> x4, Pallas kernels: none -> 69.6 us  [the longest x1 38.1 us: hidden_rows(): pl.pallas_call(functools.partial(hidden_kernel, dims, width), in_specs=[V...]
    all_to_all x1 -> x0, blocking collectives: 41 us -> none  [shards(): lax.all_to_all(outgoing, 'ep', split_axis=0, concat_axis=0, tiled=True)]
    psum x1 -> x0, waiting for transfers between devices: 20 us -> none  [shards(): lax.psum(partial_dense.astype(jnp.bfloat16), 'tp').astype(jnp.float32)]
    reduce_scatter x2 -> x0, waiting for transfers between devices: 17.4 us -> none  [the longest x1 10.3 us: shards(): lax.psum_scatter(stacked.astype(jnp.bfloat16), 'tp', scatter_dimension=2,...]
    unnamed x49 -> x30, local copies, waits for them, and re-layouts: 15.8 us -> 1.28 us
    all_to_all x2 -> x0, starting transfers between devices: 13.6 us -> none  [the longest x1 6.83 us: shards(): lax.all_to_all(inner_cols, 'ep', split_axis=0, concat_axis=1, tiled=True)]
    dot_general x10 -> x6, matrix products: 21.6 us -> 9.81 us  [the longest x1 3.7 us: shards(): jnp.dot(dense_rows, shared_down_weight, preferred_element_type=jnp.float32)]
    all_to_all x2 -> x0, waiting for transfers between devices: 8.24 us -> none  [the longest x1 8.24 us: shards(): lax.all_to_all(inner_cols, 'ep', split_axis=0, concat_axis=1, tiled=True)]
  transfers between devices with their start and end apart: 6 -> 0, of which waited for: 5 -> 0; matrix products, arithmetic and copies ran while one was open for 13% -> 0% of each run, Pallas kernels for 0% -> 0%
where the time goes in v1:
time: 124 us; the launch traced here: 122 us
  Pallas kernels  69.6 us (56%)
  other arithmetic  18.8 us (15%)
  matrix products  18.7 us (15%)
  local copies, waits for them, and re-layouts  11.2 us (9%)
  blocking collectives  2.63 us (2%)
    pallas_call x1, Pallas kernels, hidden_rows(): pl.pallas_call(functools.partial(hidden_kernel, dims, width), in_specs=[V...  38.1 us
    pallas_call x1, Pallas kernels, return_rows(): pl.pallas_call(functools.partial(return_kernel, n), in_specs=[VMEM] * 3,...  19.7 us
    pallas_call x1, Pallas kernels, mixer(): pl.pallas_call(functools.partial(mixer_kernel, channels), grid=(width //...  7.47 us
    pallas_call x1, Pallas kernels, pair_swap(): pl.pallas_call(functools.partial(pair_kernel, count), in_specs=[VMEM] * c...  4.33 us
    dynamic_slice x5, local copies, waits for them, and re-layouts, own_rows(): return lax.dynamic_slice_in_dim(values, column_start, half_width, 0)  4.12 us
    dot_general x1, matrix products, shards(): jnp.dot(dense_rows, shared_down_weight, preferred_element_type=jnp.float32)  3.7 us
    convert_element_type x2, other arithmetic, mixer(): o.reshape(width, states).astype(jnp.bfloat16)  3.57 us
    dot_general x1, matrix products, shards(): jnp.dot(inner, expert_down_weight[0], preferred_element_type=jnp.float32)  3.32 us

profile of v1, /device:TPU:0, one launch (start us, length us, event | category | flops | bytes accessed | tf_op | source)
XLA Modules:
  0.0 121.8 jit_solution(1636298105544539730)
XLA Ops:
  0.7 0.8 exp.28
  1.5 1.1 fusion.24
  2.6 2.6 %psum.7 = f32[64]{0:T(128)S(1)} all-reduce(f32[64]{0:T(128)S(1)} %fusion.24), channel_id=1, replica_groups=mesh['ep'=16,'tp'=2] {'tp'}, use_global_device_ids=true, to_apply=%region_1.2 | all-reduce | flops 64 | bytes 512 | tf_op jit(solution)/shard_map/psum | solution.py:348
  5.2 0.7 and_select_fusion
  5.9 0.7 fusion.46
  6.6 0.7 dynamic_slice.88
  7.3 0.7 dynamic_slice.34
  8.0 1.3 %dynamic_slice.37 = f32[1024]{0:T(1024)} dynamic-slice(f32[2048]{0:T(1024)} %param.29, s32[]{:T(128)S(6)} %select_n.81), dynamic_slice_sizes={1024} | dynamic-slice | bytes 8196 | tf_op jit(solution)/shard_map/dynamic_slice | solution.py:330
  9.3 0.1 copy.62
  9.4 0.7 constant_dynamic-slice_fusion.3
  10.1 0.8 constant_dynamic-slice_fusion.2
  10.9 0.1 fusion.60
  11.0 0.6 pad.9.ranks_ref
  11.7 1.7 %fusion.26.normed_ref = bf16[64,1024]{1,0:T(8,128)(2,1)} fusion(bf16[64,1024]{1,0:T(8,128)(2,1)} %tokens_ref.1, f32[1024]{0:T(1024)S(1)} %dynamic_slice.34, f32[64]{0:T(128)S(1)} %add_rsqrt_fusion), kind=kLoop, calls=%fused_computation.47 | loop fusion | flops 262144 | bytes 266496 | tf_op jit(solution)/shard_map/convert_element_type | solution.py:350
  13.3 1.6 %fusion.42 = (f32[64,64]{1,0:T(8,128)S(1)}, f32[64,64]{1,0:T(8,128)}, f32[64,64]{1,0:T(8,128)}, f32[64,64]{1,0:T(8,128)S(1)}) fusion(f32[64,64]{1,0:T(8,128)} %param.31, f32[64,64]{1,0:T(8,128)} %param.30, f32[64]{0:T(128)S(1)} %exp.28), kind=kLoop, calls=%fused_computation.72 | loop fusion | flops 73728 | bytes 98560 | tf_op jit(solution)/shard_map/div | solution.py:26
  14.9 0.2 copy.61
  15.1 0.8 pad.8.router_ref
  15.9 1.8 %convert_element_type.108 = bf16[64,16,64]{2,1,0:T(8,128)(2,1)} convert(f32[64,16,64]{2,1,0:T(8,128)} %param.35) | non-fusion elementwise | flops 65536 | bytes 393216 | tf_op jit(solution)/shard_map/convert_element_type | solution.py:76
  17.7 1.8 %convert_element_type.110 = bf16[64,16,64]{2,1,0:T(8,128)(2,1)} convert(f32[64,16,64]{2,1,0:T(8,128)} %param.36) | non-fusion elementwise | flops 65536 | bytes 393216 | tf_op jit(solution)/shard_map/convert_element_type | solution.py:76
  19.5 0.9 add_convert_fusion
  20.4 7.5 %mixer.1 = (bf16[64,1024]{1,0:T(8,128)(2,1)}, f32[64,64,64]{2,1,0:T(8,128)}, f32[64,64,64]{2,1,0:T(8,128)}) custom-call(bf16[64,1024]{1,0:T(8,128)(2,1)} %fusion.26.normed_ref, f32[64,64,64]{2,1,0:T(8,128)} %re_ref.1, f32[64,64,64]{2,1,0:T(8,128)} %im_ref.1, f32[64,64]{1,0:T(8,128)} %get-tuple-element.35.ar_ref, f32[64,64]{1,0:T(8,128)} %get-tuple-element.34.ai_ref, ...), custom_call_target="tpu_custom_call" | custom-call | tf_op jit(solution)/shard_map/mixer/pallas_call | solution.py:81
  27.9 3.2 %fusion.1 = bf16[1,64,2048]{2,1,0:T(8,128)(2,1)S(1)} fusion(bf16[64,1024]{1,0:T(8,128)(2,1)} %get-tuple-element.14, bf16[1024,2048]{1,0:T(8,128)(2,1)} %param.39), kind=kOutput, calls=%fused_computation.4 | convolution fusion | flops 268566528 | bytes 4587520 | tf_op jit(solution)/shard_map/dot_general | solution.py:357
  31.2 0.2 copy-done.2
  31.4 0.8 fusion
  32.3 0.9 fusion.31
  33.1 38.1 %hidden_rows.1 = (bf16[64,1024]{1,0:T(8,128)(2,1)}, f32[64,128]{1,0:T(8,128)}, bf16[4,2,2,64,1024]{4,3,2,1,0:T(8,128)(2,1)}, bf16[4,2,2,64,128]{4,3,2,1,0:T(8,128)(2,1)}) custom-call(bf16[2,64,1024]{2,1,0:T(8,128)(2,1)} %get-tuple-element.32.keep_ref, bf16[2,64,1024]{2,1,0:T(8,128)(2,1)} %get-tuple-element.31.send_ref, bf16[64,1024]{1,0:T(8,128)(2,1)} %tokens_ref.1, ...), custom_call_target="tpu_custom_call" | custom-call | tf_op jit(solution)/shard_map/hidden_rows/pallas_call | solution.py:207
  71.2 0.9 slice_reduce_fusion
  72.1 0.9 fusion.45
  73.0 1.0 fusion.43
  74.0 1.2 select_reduce_fusion
  75.3 0.8 fusion.44
  76.2 0.8 slice.18
  77.2 2.4 %convolution_convert_fusion.4 = bf16[1024,128]{1,0:T(8,128)(2,1)S(1)} fusion(bf16[1024,1024]{1,0:T(8,128)(2,1)} %bitcast.76, bf16[1024,128]{1,0:T(8,128)(2,1)S(1)} %copy-done.10), kind=kOutput, calls=%fused_computation.13 | convolution fusion | flops 268566528 | bytes 2621440 | tf_op jit(solution)/shard_map/dot_general | solution.py:387
  79.7 0.7 convolution_convert_fusion.5
  80.4 1.5 %convolution_convert_fusion.3.refs_0_ = bf16[256,1024]{1,0:T(8,128)(2,1)} fusion(bf16[1024,1024]{1,0:T(8,128)(2,1)S(1)} %bitcast.78, s32[1024]{0:T(1024)S(1)} %fusion.50), kind=kOutput, calls=%fused_computation.10 | convolution fusion | flops 537395200 | bytes 2625536 | tf_op jit(solution)/shard_map/dot_general | solution.py:379
  81.9 0.7 fusion.30.refs_1_
  82.7 4.3 %pair_swap.1 = (bf16[256,1024]{1,0:T(8,128)(2,1)}, bf16[2,16,32,128]{3,2,1,0:T(8,128)(2,1)}) custom-call(bf16[256,1024]{1,0:T(8,128)(2,1)} %convolution_convert_fusion.3.refs_0_, bf16[2,16,32,128]{3,2,1,0:T(8,128)(2,1)} %fusion.30.refs_1_), custom_call_target="tpu_custom_call" | custom-call | tf_op jit(solution)/shard_map/pair_swap/pallas_call | solution.py:122
  87.0 1.2 convert_add_fusion
  88.2 0.7 fusion.36.dense_ref
  89.1 0.8 copy-done.7
  89.8 0.2 copy-done.8
  90.0 1.5 %fusion.5 = f32[256,512]{1,0:T(8,128)} fusion(bf16[1,2048,512]{2,1,0:T(8,128)(2,1)S(1)} %copy-done.14, bf16[256,1024]{1,0:T(8,128)(2,1)S(1)} %get-tuple-element.30, bf16[256,1024]{1,0:T(8,128)(2,1)S(1)} %get-tuple-element.29), kind=kOutput, calls=%fused_computation.8 | convolution fusion | flops 538968064 | bytes 3670016 | tf_op jit(solution)/shard_map/dot_general | solution.py:402
  91.6 3.3 %convolution_convert_fusion = bf16[256,2048]{1,0:T(8,128)(2,1)S(1)} fusion(bf16[1,512,2048]{2,1,0:T(8,128)(2,1)S(1)} %copy-done, bf16[1,2048,512]{2,1,0:T(8,128)(2,1)} %param.45, bf16[256,1024]{1,0:T(8,128)(2,1)} %copy-done.8, bf16[256,1024]{1,0:T(8,128)(2,1)} %copy-done.7, f32[256,512]{1,0:T(8,128)} %fusion.5), kind=kOutput, calls=%fused_computation | convolution fusion | flops 1077149696 | bytes 6815744 | tf_op jit(solution)/shard_map/dot_general | solution.py:405
  94.9 1.1 constant_dynamic-slice_fusion
  96.0 19.7 %return_rows.1 = (bf16[16,16,1024]{2,1,0:T(8,128)(2,1)}, bf16[2,16,32,128]{3,2,1,0:T(8,128)(2,1)}) custom-call(bf16[16,16,1024]{2,1,0:T(8,128)(2,1)} %get-tuple-element.28.keep_ref, bf16[16,16,1024]{2,1,0:T(8,128)(2,1)} %get-tuple-element.27.give_ref, bf16[16,32,128]{2,1,0:T(8,128)(2,1)} %fusion.36.dense_ref), custom_call_target="tpu_custom_call" | custom-call | tf_op jit(solution)/shard_map/return_rows/pallas_call | solution.py:277
  115.7 1.3 %fusion.14 = f32[64,1024]{1,0:T(8,128)S(1)} fusion(bf16[16,16,1024]{2,1,0:T(8,128)(2,1)} %get-tuple-element.21, bf16[64,1024]{1,0:T(8,128)(2,1)S(1)} %copy-done.12, bf16[64,16]{0,1:T(8,128)(2,1)S(1)} %select_reduce_fusion.1, f32[64,16]{0,1:T(8,128)S(1)} %copy.64, f32[16]{0:T(128)S(1)} %iota_add_fusion), kind=kOutput, calls=%fused_computation.18 | convolution fusion | flops 33718272 | bytes 923712 | tf_op jit(solution)/shard_map/dot_general | solution.py:419
  117.1 1.1 copy.72
  118.1 3.7 %fusion.15 = bf16[64,1024]{1,0:T(8,128)(2,1)} fusion(f32[64,1024]{1,0:T(8,128)S(1)} %fusion.14, bf16[2048,1024]{1,0:T(8,128)(2,1)} %param.49, bf16[8,8,16,128]{3,2,1,0:T(8,128)(2,1)S(1)} %bitcast.87, f32[64]{0:T(128)S(1)} %fusion.43), kind=kOutput, calls=%fused_computation.19 | convolution fusion | flops 268632064 | bytes 4849920 | tf_op jit(solution)/shard_map/dot_general | solution.py:423
  (45 shorter events, 0.6 us)
Async XLA Ops:
  0.6 90.9 %copy-start = (bf16[1,512,2048]{2,1,0:T(8,128)(2,1)S(1)}, bf16[1,512,2048]{2,1,0:T(8,128)(2,1)}, u32[]{:S(2)}) copy-start(bf16[1,512,2048]{2,1,0:T(8,128)(2,1)} %param.46) | copy-start | bytes 6291460
  0.6 18.8 %copy-start.5 = (f32[64,64,16]{1,2,0:T(8,128)S(1)}, f32[64,64,16]{1,2,0:T(8,128)}, u32[]{:S(2)}) copy-start(f32[64,64,16]{1,2,0:T(8,128)} %param.34) | copy-start | bytes 786436
  0.7 18.8 %copy-start.4 = (f32[64,64,16]{1,2,0:T(8,128)S(1)}, f32[64,64,16]{1,2,0:T(8,128)}, u32[]{:S(2)}) copy-start(f32[64,64,16]{1,2,0:T(8,128)} %param.33) | copy-start | bytes 786436
  27.9 3.5 %copy-start.2 = (bf16[1024,2048]{1,0:T(8,128)(2,1)S(1)}, bf16[1024,2048]{1,0:T(8,128)(2,1)}, u32[]{:S(2)}) copy-start(bf16[1024,2048]{1,0:T(8,128)(2,1)} %param.38) | copy-start | bytes 12582916
  27.9 3.5 %copy-start.9 = (bf16[64,1024]{1,0:T(8,128)(2,1)S(1)}, bf16[64,1024]{1,0:T(8,128)(2,1)}, u32[]{:S(2)}) copy-start(bf16[64,1024]{1,0:T(8,128)(2,1)} %get-tuple-element.14) | copy-start | bytes 393220
  32.3 44.9 %copy-start.13 = (s32[64,2]{0,1:T(2,128)S(1)}, s32[64,2]{0,1:T(2,128)}, u32[]{:S(2)}) copy-start(s32[64,2]{0,1:T(2,128)} %param.43) | copy-start | bytes 1540
  32.3 45.0 %copy-start.10 = (bf16[1024,128]{1,0:T(8,128)(2,1)S(1)}, bf16[1024,128]{1,0:T(8,128)(2,1)}, u32[]{:S(2)}) copy-start(bf16[1024,128]{1,0:T(8,128)(2,1)} %param.48) | copy-start | bytes 786436
  33.1 46.6 %copy-start.11 = (bf16[1024,128]{1,0:T(8,128)(2,1)S(1)}, bf16[1024,128]{1,0:T(8,128)(2,1)}, u32[]{:S(2)}) copy-start(bf16[1024,128]{1,0:T(8,128)(2,1)} %param.47) | copy-start | bytes 786436
  77.2 2.5 %copy-start.1 = (bf16[4,2,2,64,1024]{4,3,2,1,0:T(8,128)(2,1)S(1)}, bf16[4,2,2,64,1024]{4,3,2,1,0:T(8,128)(2,1)}, u32[]{:S(2)}) copy-start(bf16[4,2,2,64,1024]{4,3,2,1,0:T(8,128)(2,1)} %get-tuple-element.18) | copy-start | bytes 6291460
  81.9 7.0 %copy-start.3 = (bf16[256,1024]{1,0:T(8,128)(2,1)S(1)}, bf16[256,1024]{1,0:T(8,128)(2,1)}, u32[]{:S(2)}) copy-start(bf16[256,1024]{1,0:T(8,128)(2,1)} %convolution_convert_fusion.3.refs_0_) | copy-start | bytes 1572868
  87.0 1.9 %copy-start.6 = (bf16[256,1024]{1,0:T(8,128)(2,1)S(1)}, bf16[256,1024]{1,0:T(8,128)(2,1)}, u32[]{:S(2)}) copy-start(bf16[256,1024]{1,0:T(8,128)(2,1)} %get-tuple-element.19) | copy-start | bytes 1572868
  87.0 3.0 %copy-start.14 = (bf16[1,2048,512]{2,1,0:T(8,128)(2,1)S(1)}, bf16[1,2048,512]{2,1,0:T(8,128)(2,1)}, u32[]{:S(2)}) copy-start(bf16[1,2048,512]{2,1,0:T(8,128)(2,1)} %param.44) | copy-start | bytes 6291460
  89.0 0.8 copy-start.7
  89.0 1.0 copy-start.8
  94.9 20.8 %copy-start.12 = (bf16[64,1024]{1,0:T(8,128)(2,1)S(1)}, bf16[64,1024]{1,0:T(8,128)(2,1)}, u32[]{:S(2)}) copy-start(bf16[64,1024]{1,0:T(8,128)(2,1)} %get-tuple-element.15) | copy-start | bytes 393220

commit v2 on v1

--- a/solution.py
+++ b/solution.py
@@ -59,8 +59,8 @@
     dims = (((1,), (1,)), ((), ()))
     flat_re = n_re.reshape(rows * groups, states).astype(jnp.bfloat16)
     flat_im = n_im.reshape(rows * groups, states).astype(jnp.bfloat16)
-    read = lax.dot_general(flat_re, cr_ref[...], dims, preferred_element_type=jnp.float32)
-    read = read - lax.dot_general(flat_im, ci_ref[...], dims, preferred_element_type=jnp.float32)
+    read = lax.dot_general(flat_re, cr_ref[...].astype(jnp.bfloat16), dims, preferred_element_type=jnp.float32)
+    read = read - lax.dot_general(flat_im, ci_ref[...].astype(jnp.bfloat16), dims, preferred_element_type=jnp.float32)
     mixed = jnp.sum(read.reshape(rows, groups, lanes) * mask[None], axis=1) + skip_ref[...] * u
     act_ref[...] = jax.nn.gelu(mixed).astype(jnp.bfloat16)
 
@@ -73,7 +73,7 @@
     per = LANES // channels
     maps = [
         jnp.swapaxes(b, 1, 2).reshape(width, states).astype(jnp.bfloat16) for b in (bbar_re, bbar_im)
-    ] + [o.reshape(width, states).astype(jnp.bfloat16) for o in (out_re, out_im)]
+    ] + [o.reshape(width, states) for o in (out_re, out_im)]
     cols = pl.BlockSpec((rows, LANES), lambda i: (0, i))
     state = pl.BlockSpec((rows, per, states), lambda i: (0, i, 0))
     abar = pl.BlockSpec((per, states), lambda i: (i, 0))
@@ -137,85 +137,137 @@
 
 
 def hidden_kernel(
-    dims, width, keep_ref, send_ref, tokens_ref, gain_ref, router_ref, ranks_ref,
+    dims, width, keep_ref, send_ref, tokens_ref, gain_ref, group_ref, expert_ref, blend_ref, ranks_ref, named_ref,
     hidden_ref, stats_ref, rows_ref, rank_out_ref,
-    vg_buf, stat_buf, stat_in, pair_send, pair_recv, send, recv,
+    vg_buf, router, stat_buf, stat_in, pair_send, pair_recv, send, recv,
 ):
     ep, tp = lax.axis_index("ep"), lax.axis_index("tp")
     me = (ep // (dims[1] * dims[2]), (ep // dims[2]) % dims[1], ep % dims[2])
     partner = (ep, 1 - tp)
+    rows, half = tokens_ref.shape
+    experts = expert_ref.shape[0]
+    paths = [(rows_ref, lo * LANES, n * LANES, order) for lo, n, order in gather_plan(half // LANES) if n]
+    paths = [(rank_out_ref, 0, LANES, (2, 1, 0))] + paths
 
     def neighbour(dim, step):
         c = [me[d] if d != dim else lax.rem(me[d] + step, dims[d]) for d in range(3)]
         return ((c[0] * dims[1] + c[1]) * dims[2] + c[2], tp)
+
+    sent = {}
+
+    def give(p, level, *offsets):
+        ref, lo, n, order = paths[p]
+        spot = list(me)
+        for d, o in zip(order, offsets):
+            spot[d] = lax.rem(me[d] + dims[d] - o, dims[d])
+        block = ref.at[spot[0], spot[1], spot[2], :, pl.ds(lo, n)]
+        for step in range(1, dims[order[level]]):
+            key = (p,) + offsets + (step,)
+            at = len(sent)
+            copy = remote(block, block, send.at[at], recv.at[at], neighbour(order[level], step))
+            copy.start()
+            sent[key] = copy
 
     greet([partner] + [neighbour(d, s) for d in range(3) for s in range(1, dims[d])])
     swap = remote(send_ref, vg_buf, pair_send.at[0], pair_recv.at[0], partner)
     swap.start()
     rank_out_ref[me[0], me[1], me[2]] = ranks_ref[...]
+    mine = pl.ds(pl.multiple_of(tp * half, LANES), half)
+    groups = group_ref.shape[0]
+    router[...] = jnp.zeros_like(router)
+    router[0:experts] = expert_ref[:, mine].astype(jnp.float32)
+    router[experts:experts + groups] = group_ref[:, mine].astype(jnp.float32)
+    router[experts + groups:experts + groups + 1] = blend_ref[:, mine]
+    stat_buf[...] = jnp.zeros_like(stat_buf)
     swap.wait()
-    rows, half = tokens_ref.shape
     value = keep_ref[0].astype(jnp.float32) + vg_buf[0].astype(jnp.float32)
     gate = keep_ref[1].astype(jnp.float32) + vg_buf[1].astype(jnp.float32)
     mix = (value * jax.nn.sigmoid(gate)).astype(jnp.bfloat16).astype(jnp.float32)
     hidden = (tokens_ref[...].astype(jnp.float32) + mix).astype(jnp.bfloat16)
     hidden_ref[...] = hidden
     hidden = hidden.astype(jnp.float32)
-    scaled = hidden * gain_ref[...]
-    raw = jnp.dot(scaled.astype(jnp.bfloat16), router_ref[...], preferred_element_type=jnp.float32)
-    squares = jnp.sum(hidden * hidden, axis=1, keepdims=True)
-    lane = lax.broadcasted_iota(jnp.int32, raw.shape, 1)
-    stat_buf[...] = jnp.where(lane == LANES - 1, squares, raw)
+    scaled = hidden * gain_ref[:, mine]
+    raw = lax.dot_general(
+        scaled.astype(jnp.bfloat16), router[...].astype(jnp.bfloat16), (((1,), (1,)), ((), ())),
+        preferred_element_type=jnp.float32,
+    )
+    stat_buf[:, 0:router.shape[0]] = raw
+    stat_buf[:, LANES - 1:LANES] = jnp.sum(hidden * hidden, axis=1, keepdims=True)
     swap = remote(stat_buf, stat_in, pair_send.at[1], pair_recv.at[1], partner)
     swap.start()
     swap.wait()
     total = stat_buf[...] + stat_in[...]
     inverse = lax.rsqrt(total[:, LANES - 1:] / width + EPS)
-    stats_ref[...] = total * inverse
     rows_ref[me[0], me[1], me[2]] = (scaled * inverse).astype(jnp.bfloat16)
 
-    paths = [(rows_ref, lo * LANES, n * LANES, order) for lo, n, order in gather_plan(half // LANES) if n]
-    paths = [(rank_out_ref, 0, LANES, (2, 1, 0))] + paths
-    slots = sum(d - 1 for d in dims)
-    pending = [[] for _ in paths]
-    for stage in range(3):
-        for p, (ref, lo, n, order) in enumerate(paths):
-            for copy in pending[p]:
-                copy.wait_recv()
-            dim = order[stage]
-            done = order[:stage]
-            where = tuple(pl.ds(0, dims[d]) if d in done else pl.ds(me[d], 1) for d in range(3))
-            block = ref.at[where + (pl.ds(0, rows), pl.ds(lo, n))]
-            base = p * slots + sum(dims[d] - 1 for d in done)
-            fresh = [
-                remote(block, block, send.at[base + s - 1], recv.at[base + s - 1], neighbour(dim, s))
-                for s in range(1, dims[dim])
-            ]
-            for copy in fresh:
-                copy.start()
-            for copy in pending[p]:
-                copy.wait_send()
-            pending[p] = fresh
-    for copies in pending:
-        for copy in copies:
-            copy.wait()
-
-
-def hidden_rows(dims, width, keep, give, tokens, gain, router, ranks):
+    every = range(len(paths))
+    size = [[dims[d] for d in path[3]] for path in paths]
+    for p in every:
+        give(p, 0)
+    for p in every:
+        give(p, 1, 0)
+    for p in every:
+        give(p, 2, 0, 0)
+    for p in every:
+        for b in range(1, size[p][1]):
+            sent[(p, 0, b)].wait_recv()
+            give(p, 2, 0, b)
+    for a in sorted(range(1, max(dims)), key=lambda o: min(o, max(dims) - o)):
+        for p in every:
+            if a < size[p][0]:
+                sent[(p, a)].wait_recv()
+                give(p, 1, a)
+                give(p, 2, a, 0)
+    for a in sorted(range(1, max(dims)), key=lambda o: min(o, max(dims) - o)):
+        for p in every:
+            if a < size[p][0]:
+                for b in range(1, size[p][1]):
+                    sent[(p, a, b)].wait_recv()
+                    give(p, 2, a, b)
+
+    logits = total * inverse
+    lane = lax.broadcasted_iota(jnp.int32, logits.shape, 1)
+    named = named_ref[...] > 0
+    is_group = (lane >= experts) & (lane < experts + groups)
+    low = jnp.full_like(logits, -jnp.inf)
+    group_exp = jnp.exp(logits - jnp.max(jnp.where(is_group, logits, low), axis=1, keepdims=True))
+    group_exp = jnp.where(is_group, group_exp, 0.0)
+    group_prob = group_exp / jnp.sum(group_exp, axis=1, keepdims=True)
+    top = jnp.max(jnp.where(named, logits, low), axis=1, keepdims=True)
+    chosen = jnp.where(named, jnp.exp(jnp.where(named, logits - top, 0.0)), 0.0)
+    chosen = chosen / jnp.sum(chosen, axis=1, keepdims=True)
+    per_group = experts // groups
+    spread = jnp.zeros_like(logits)
+    for g in range(groups):
+        inside = (lane >= g * per_group) & (lane < (g + 1) * per_group)
+        spread = jnp.where(inside, group_prob[:, experts + g:experts + g + 1], spread)
+    stats_ref[...] = jnp.where(named, chosen * spread, jax.nn.sigmoid(logits))
+
+    for key, copy in sent.items():
+        if len(key) == 4:
+            copy.wait_recv()
+    for copy in sent.values():
+        copy.wait_send()
+
+
+def hidden_rows(dims, width, keep, give, tokens, gain, group_map, expert_map, blend_map, ranks, named):
     rows, half = tokens.shape
-    slots = 4 * sum(d - 1 for d in dims)
+    experts = expert_map.shape[0]
+    slots = 4 * (dims[0] * dims[1] * dims[2] - 1)
+    routers = -(-(experts + group_map.shape[0] + 1) // 8) * 8
     return pl.pallas_call(
         functools.partial(hidden_kernel, dims, width),
-        in_specs=[VMEM] * 6,
+        in_specs=[VMEM] * 9,
         out_specs=[VMEM] * 4,
         out_shape=[
             jax.ShapeDtypeStruct((rows, half), jnp.bfloat16),
             jax.ShapeDtypeStruct((rows, LANES), jnp.float32),
             jax.ShapeDtypeStruct(dims + (rows, half), jnp.bfloat16),
-            jax.ShapeDtypeStruct(dims + (rows, LANES), jnp.bfloat16),
+            jax.ShapeDtypeStruct(dims + (experts, LANES), jnp.float32),
         ],
         scratch_shapes=[
             pltpu.VMEM((2, rows, half), jnp.bfloat16),
+            pltpu.VMEM((routers, half), jnp.float32),
             pltpu.VMEM((rows, LANES), jnp.float32),
             pltpu.VMEM((rows, LANES), jnp.float32),
             pltpu.SemaphoreType.DMA((2,)),
@@ -225,7 +277,7 @@
         ],
         compiler_params=pltpu.CompilerParams(collective_id=2, has_side_effects=True),
         name="hidden_rows",
-    )(keep, give, tokens, gain, router, ranks)
+    )(keep, give, tokens, gain, group_map, expert_map, blend_map, ranks, named)
 
 
 def return_kernel(
@@ -234,7 +286,7 @@
 ):
     ep, tp = lax.axis_index("ep"), lax.axis_index("tp")
     partner = (ep, 1 - tp)
-    peers = [lax.rem(ep + s, n) for s in range(1, n)]
+    peers = [lax.rem(ep + s, n) for s in sorted(range(1, n), key=lambda o: abs(2 * o - n))]
     greet([partner] + [(q, tp) for q in peers])
     swap = remote(give_ref, got, pair_send.at[0], pair_recv.at[0], partner)
     swap.start()
@@ -334,7 +386,6 @@
 
     experts = expert_router_weight.shape[1]
     top_count = routes.shape[1]
-    per_group = experts // NG
     capacity = max(2, 2 * seq_rows * top_count // experts)
     hits = routes[:, :, None] == jnp.arange(experts, dtype=jnp.int32)[None, None, :]
     named = jnp.any(hits, axis=1)
@@ -342,7 +393,8 @@
     earlier = (order[None, :] <= order[:, None]).astype(jnp.bfloat16)
     counted = jnp.dot(earlier, named.astype(jnp.bfloat16), preferred_element_type=jnp.float32)
     ranks_f32 = jnp.where(named, counted, 0.0)
-    ranks = jnp.pad(ranks_f32.astype(jnp.bfloat16), ((0, 0), (0, LANES - experts)))
+    ranks = jnp.pad(ranks_f32.T, ((0, 0), (0, LANES - seq_rows)))
+    named_lanes = jnp.pad(named.astype(jnp.float32), ((0, 0), (0, LANES - experts)))
 
     float_tokens = tokens.astype(jnp.float32)
     square_sum = lax.psum(jnp.sum(float_tokens * float_tokens, axis=1), "tp")
@@ -356,25 +408,17 @@
     value_part = jnp.dot(activated, mixer_value_weight, preferred_element_type=jnp.float32)
     gate_part = jnp.dot(activated, mixer_gate_weight, preferred_element_type=jnp.float32)
     stacked = jnp.stack([value_part.astype(jnp.bfloat16), gate_part.astype(jnp.bfloat16)], axis=0)
-    router_map = jnp.concatenate(
-        [
-            own_rows(group_router_weight),
-            own_rows(expert_router_weight),
-            own_rows(dense_blend_weight).astype(jnp.bfloat16)[:, None],
-        ],
-        axis=1,
-    )
-    router_map = jnp.pad(router_map, ((0, 0), (0, LANES - router_map.shape[1])))
     hidden, stats, gathered, gathered_ranks = hidden_rows(
         ep_dims(ep_count), width, own_cols(stacked, tp), own_cols(stacked, 1 - tp), tokens,
-        own_rows(expert_norm_gain)[None, :], router_map, ranks,
+        expert_norm_gain[None, :], group_router_weight.T, expert_router_weight.T, dense_blend_weight[None, :],
+        ranks, named_lanes,
     )
     rows = gathered.reshape(ep_count * seq_rows, half_width)
-    rank_rows = gathered_ranks.reshape(ep_count * seq_rows, LANES)
-    lane = jnp.arange(LANES, dtype=jnp.int32)[None, :]
-    mine = jnp.sum(jnp.where(lane == ep, rank_rows.astype(jnp.float32), 0.0), axis=1).astype(jnp.int32)
-    source = jnp.arange(ep_count * seq_rows, dtype=jnp.int32) // seq_rows
-    slot = jnp.where(mine > 0, source * capacity + mine - 1, -1)
+    mine = lax.dynamic_index_in_dim(
+        gathered_ranks.reshape(ep_count, experts, LANES), ep, 1, keepdims=False
+    )[:, :seq_rows].astype(jnp.int32)
+    source = jnp.arange(ep_count, dtype=jnp.int32)[:, None]
+    slot = jnp.where(mine > 0, source * capacity + mine - 1, -1).reshape(-1)
     dispatch = slot[None, :] == jnp.arange(ep_count * capacity, dtype=jnp.int32)[:, None]
     half_rows = jnp.dot(
         dispatch.astype(jnp.bfloat16), rows, preferred_element_type=jnp.float32
@@ -406,13 +450,7 @@
     part_out = part_out.reshape(ep_count, capacity, width)
     returned, dense_all = return_rows(own_cols(part_out, tp), own_cols(part_out, 1 - tp), dense_inner)
 
-    logits, blend_logit = stats[:, :NG + experts], stats[:, NG + experts]
-    group_prob = jax.nn.softmax(logits[:, :NG], axis=-1)
-    chosen = jnp.sum(jnp.where(hits, logits[:, None, NG:], 0.0), axis=2)
-    group_hits = (routes // per_group)[:, :, None] == jnp.arange(NG, dtype=jnp.int32)[None, None, :]
-    group_sel = jnp.sum(jnp.where(group_hits, group_prob[:, None, :], 0.0), axis=2)
-    weights = jax.nn.softmax(chosen, axis=1) * group_sel
-    expert_weight = jnp.sum(jnp.where(hits, weights[:, :, None], 0.0), axis=1)
+    expert_weight, blend = stats[:, :experts], stats[:, experts + NG]
     places = jnp.arange(capacity, dtype=jnp.float32) + 1.0
     combine = jnp.where(ranks_f32[:, :, None] == places[None, None, :], expert_weight[:, :, None], 0.0)
     combine = combine.reshape(seq_rows, experts * capacity).astype(jnp.bfloat16)
@@ -421,7 +459,7 @@
     )
     dense_rows = jnp.transpose(dense_all, (0, 2, 1, 3)).reshape(seq_rows, ep_count * dense_cols)
     dense_out = jnp.dot(dense_rows, shared_down_weight, preferred_element_type=jnp.float32)
-    result = hidden.astype(jnp.float32) + routed + jax.nn.sigmoid(blend_logit)[:, None] * dense_out
+    result = hidden.astype(jnp.float32) + routed + blend[:, None] * dense_out
     return (result.astype(jnp.bfloat16), next_re, next_im)
 
 

time: 124 us -> 111 us (0.90)
  other arithmetic: 18.8 us -> 11.4 us
  local copies, waits for them, and re-layouts: 11.2 us -> 8.29 us
  Pallas kernels: 69.6 us -> 68.1 us
    pallas_call x1, Pallas kernels: 38.1 us -> 32.2 us  [hidden_rows(): pl.pallas_call(functools.partial(hidden_kernel, dims, width), in_specs=[V...]
    pallas_call x1, Pallas kernels: 19.7 us -> 24.1 us  [return_rows(): pl.pallas_call(functools.partial(return_kernel, n), in_specs=[VMEM] * 3,...]
    convert_element_type x3 -> x0, other arithmetic: 3.57 us -> none  [the longest x2 3.57 us: mixer(): o.reshape(width, states).astype(jnp.bfloat16)]
    dynamic_slice x5 -> x1, local copies, waits for them, and re-layouts: 4.12 us -> 0.69 us  [own_rows(): return lax.dynamic_slice_in_dim(values, column_start, half_width, 0)]
    reduce_sum x6 -> x0, other arithmetic: 2.2 us -> none  [the longest x1 1.17 us: shards(): jnp.sum(jnp.where(lane == ep, rank_rows.astype(jnp.float32), 0.0), axis=1)]
    div x2 -> x0, other arithmetic: 1.8 us -> none  [the longest x1 0.96 us: shards(): jax.nn.sigmoid(blend_logit)[:, None] * dense_out]
where the time goes in v2:
time: 111 us; the launch traced here: 110 us
  Pallas kernels  68.1 us (61%)
  matrix products  18.8 us (17%)
  other arithmetic  11.4 us (10%)
  local copies, waits for them, and re-layouts  8.29 us (7%)
  blocking collectives  2.63 us (2%)
    pallas_call x1, Pallas kernels, hidden_rows(): pl.pallas_call(functools.partial(hidden_kernel, dims, width), in_specs=[V...  32.2 us
    pallas_call x1, Pallas kernels, return_rows(): pl.pallas_call(functools.partial(return_kernel, n), in_specs=[VMEM] * 3,...  24.1 us
    pallas_call x1, Pallas kernels, mixer(): pl.pallas_call(functools.partial(mixer_kernel, channels), grid=(width //...  7.51 us
    pallas_call x1, Pallas kernels, pair_swap(): pl.pallas_call(functools.partial(pair_kernel, count), in_specs=[VMEM] * c...  4.31 us
    dot_general x1, matrix products, shards(): jnp.dot(dense_rows, shared_down_weight, preferred_element_type=jnp.float32)  3.7 us
    dot_general x1, matrix products, shards(): jnp.dot(inner, expert_down_weight[0], preferred_element_type=jnp.float32)  3.32 us
    dot_general x1, matrix products, shards(): jnp.dot(activated, mixer_gate_weight, preferred_element_type=jnp.float32)  3.24 us
    dot_general x2, matrix products, shards(): jnp.dot(rows, w, preferred_element_type=jnp.float32).astype(jnp.bfloat16)  3.17 us

profile of v2, /device:TPU:0, one launch (start us, length us, event | category | flops | bytes accessed | tf_op | source)
XLA Modules:
  0.0 110.0 jit_solution(1793505165712877615)
XLA Ops:
  0.6 0.0 copy-start
  0.7 0.8 exp.14
  1.5 1.0 fusion.24
  2.5 2.6 %psum.7 = f32[64]{0:T(128)S(1)} all-reduce(f32[64]{0:T(128)S(1)} %fusion.24), channel_id=1, replica_groups=mesh['ep'=16,'tp'=2] {'tp'}, use_global_device_ids=true, to_apply=%region_1.2 | all-reduce | flops 64 | bytes 512 | tf_op jit(solution)/shard_map/psum | solution.py:400
  5.2 0.7 fusion.43
  5.8 0.7 dynamic_slice.26
  6.5 0.1 convolution_select_fusion
  6.7 0.1 copy.41
  6.8 0.6 pad.10.ranks_ref
  7.4 0.6 pad_convert_fusion.named_ref
  8.0 1.7 %fusion.26.normed_ref = bf16[64,1024]{1,0:T(8,128)(2,1)} fusion(bf16[64,1024]{1,0:T(8,128)(2,1)} %tokens_ref.1, f32[1024]{0:T(1024)S(1)} %dynamic_slice.26, f32[64]{0:T(128)S(1)} %add_rsqrt_fusion), kind=kLoop, calls=%fused_computation.46 | loop fusion | flops 262144 | bytes 266496 | tf_op jit(solution)/shard_map/convert_element_type | solution.py:402
  9.6 1.6 %fusion.42 = (f32[64,64]{1,0:T(8,128)S(1)}, f32[64,64]{1,0:T(8,128)}, f32[64,64]{1,0:T(8,128)}, f32[64,64]{1,0:T(8,128)S(1)}) fusion(f32[64,64]{1,0:T(8,128)} %param.31, f32[64,64]{1,0:T(8,128)} %param.30, f32[64]{0:T(128)S(1)} %exp.14), kind=kLoop, calls=%fused_computation.69 | loop fusion | flops 73728 | bytes 98560 | tf_op jit(solution)/shard_map/div | solution.py:26
  11.3 2.1 %add_convert_fusion = (bf16[64,64,16]{1,2,0:T(8,128)(2,1)}, bf16[64,64,16]{1,2,0:T(8,128)(2,1)}) fusion(f32[64,64,16]{1,2,0:T(8,128)} %param.33, f32[64,64,16]{1,2,0:T(8,128)} %param.34, f32[64,64]{1,0:T(8,128)S(1)} %get-tuple-element.36, f32[64,64]{1,0:T(8,128)S(1)} %get-tuple-element.33), kind=kLoop, calls=%fused_computation.38 | loop fusion | flops 524288 | bytes 819200 | tf_op jit(solution)/shard_map/convert_element_type | solution.py:75
  13.4 7.5 %mixer.1 = (bf16[64,1024]{1,0:T(8,128)(2,1)}, f32[64,64,64]{2,1,0:T(8,128)}, f32[64,64,64]{2,1,0:T(8,128)}) custom-call(bf16[64,1024]{1,0:T(8,128)(2,1)} %fusion.26.normed_ref, f32[64,64,64]{2,1,0:T(8,128)} %re_ref.1, f32[64,64,64]{2,1,0:T(8,128)} %im_ref.1, f32[64,64]{1,0:T(8,128)} %get-tuple-element.35.ar_ref, f32[64,64]{1,0:T(8,128)} %get-tuple-element.34.ai_ref, ...), custom_call_target="tpu_custom_call" | custom-call | tf_op jit(solution)/shard_map/mixer/pallas_call | solution.py:81
  20.9 0.0 copy-start.7
  20.9 3.2 %fusion.1 = bf16[1,64,2048]{2,1,0:T(8,128)(2,1)S(1)} fusion(bf16[64,1024]{1,0:T(8,128)(2,1)} %get-tuple-element.14, bf16[1024,2048]{1,0:T(8,128)(2,1)} %param.39), kind=kOutput, calls=%fused_computation.4 | convolution fusion | flops 268566528 | bytes 4587520 | tf_op jit(solution)/shard_map/dot_general | solution.py:409
  24.2 0.2 copy-done.2
  24.4 0.0 copy-done.7
  24.4 0.8 fusion
  25.3 0.0 copy-start.9
  25.3 0.9 fusion.31
  26.1 32.2 %hidden_rows.1 = (bf16[64,1024]{1,0:T(8,128)(2,1)}, f32[64,128]{1,0:T(8,128)}, bf16[4,2,2,64,1024]{4,3,2,1,0:T(8,128)(2,1)}, f32[4,2,2,16,128]{4,3,2,1,0:T(8,128)}) custom-call(bf16[2,64,1024]{2,1,0:T(8,128)(2,1)} %get-tuple-element.32.keep_ref, bf16[2,64,1024]{2,1,0:T(8,128)(2,1)} %get-tuple-element.31.send_ref, bf16[64,1024]{1,0:T(8,128)(2,1)} %tokens_ref.1, ...), custom_call_target="tpu_custom_call" | custom-call | tf_op jit(solution)/shard_map/hidden_rows/pallas_call | solution.py:258
  58.3 0.9 constant_dynamic-slice_fusion.2
  59.2 0.1 add_select_fusion
  59.2 0.1 eq.54
  59.3 0.9 slice_reduce_fusion
  60.2 0.8 slice.15
  61.0 0.1 copy.42
  61.1 2.5 %convolution_convert_fusion.4 = bf16[1024,128]{1,0:T(8,128)(2,1)S(1)} fusion(bf16[1024,1024]{1,0:T(8,128)(2,1)} %bitcast.82, bf16[1024,128]{1,0:T(8,128)(2,1)S(1)} %copy-done.8), kind=kOutput, calls=%fused_computation.13 | convolution fusion | flops 268566528 | bytes 2621440 | tf_op jit(solution)/shard_map/dot_general | solution.py:431
  63.6 0.7 convolution_convert_fusion.5
  64.3 1.5 %convolution_convert_fusion.3.refs_0_ = bf16[256,1024]{1,0:T(8,128)(2,1)} fusion(bf16[1024,1024]{1,0:T(8,128)(2,1)S(1)} %bitcast.84, s32[1024]{0:T(1024)S(1)} %eq.54), kind=kOutput, calls=%fused_computation.10 | convolution fusion | flops 537395200 | bytes 2625536 | tf_op jit(solution)/shard_map/dot_general | solution.py:423
  65.8 0.7 fusion.30.refs_1_
  66.6 4.3 %pair_swap.1 = (bf16[256,1024]{1,0:T(8,128)(2,1)}, bf16[2,16,32,128]{3,2,1,0:T(8,128)(2,1)}) custom-call(bf16[256,1024]{1,0:T(8,128)(2,1)} %convolution_convert_fusion.3.refs_0_, bf16[2,16,32,128]{3,2,1,0:T(8,128)(2,1)} %fusion.30.refs_1_), custom_call_target="tpu_custom_call" | custom-call | tf_op jit(solution)/shard_map/pair_swap/pallas_call | solution.py:122
  70.9 0.0 copy-start.11
  70.9 1.2 %convert_add_fusion = f32[2,16,32,128]{3,2,1,0:T(8,128)S(1)} fusion(bf16[2,16,32,128]{3,2,1,0:T(8,128)(2,1)} %get-tuple-element.20, s32[]{:T(128)S(6)} %select_n.61, bf16[1,16,2,32,128]{4,3,2,1,0:T(8,128)(2,1)S(1)} %bitcast.88, bf16[1,16,2,32,128]{4,3,2,1,0:T(8,128)(2,1)S(1)} %bitcast.86), kind=kLoop, calls=%fused_computation.31 | loop fusion | flops 524288 | bytes 1310724 | tf_op jit(solution)/shard_map/add | solution.py:440
  72.1 0.7 fusion.36.dense_ref
  72.8 0.0 copy-done.4
  72.8 0.1 broadcast_select_fusion.1
  72.9 0.8 copy-done.5
  73.7 0.2 copy-done.6
  73.9 1.5 %fusion.5 = f32[256,512]{1,0:T(8,128)} fusion(bf16[1,2048,512]{2,1,0:T(8,128)(2,1)S(1)} %copy-done.11, bf16[256,1024]{1,0:T(8,128)(2,1)S(1)} %get-tuple-element.30, bf16[256,1024]{1,0:T(8,128)(2,1)S(1)} %get-tuple-element.29), kind=kOutput, calls=%fused_computation.8 | convolution fusion | flops 538968064 | bytes 3670016 | tf_op jit(solution)/shard_map/dot_general | solution.py:446
  75.4 3.3 %convolution_convert_fusion = bf16[256,2048]{1,0:T(8,128)(2,1)S(1)} fusion(bf16[1,512,2048]{2,1,0:T(8,128)(2,1)S(1)} %copy-done, bf16[1,2048,512]{2,1,0:T(8,128)(2,1)} %param.45, bf16[256,1024]{1,0:T(8,128)(2,1)} %copy-done.6, bf16[256,1024]{1,0:T(8,128)(2,1)} %copy-done.5, f32[256,512]{1,0:T(8,128)} %fusion.5), kind=kOutput, calls=%fused_computation | convolution fusion | flops 1077149696 | bytes 6815744 | tf_op jit(solution)/shard_map/dot_general | solution.py:449
  78.7 0.0 copy-start.10
  78.7 1.1 constant_dynamic-slice_fusion
  79.8 24.1 %return_rows.1 = (bf16[16,16,1024]{2,1,0:T(8,128)(2,1)}, bf16[2,16,32,128]{3,2,1,0:T(8,128)(2,1)}) custom-call(bf16[16,16,1024]{2,1,0:T(8,128)(2,1)} %get-tuple-element.28.keep_ref, bf16[16,16,1024]{2,1,0:T(8,128)(2,1)} %get-tuple-element.27.give_ref, bf16[16,32,128]{2,1,0:T(8,128)(2,1)} %fusion.36.dense_ref), custom_call_target="tpu_custom_call" | custom-call | tf_op jit(solution)/shard_map/return_rows/pallas_call | solution.py:329
  103.9 1.3 %fusion.14 = f32[64,1024]{1,0:T(8,128)S(1)} fusion(bf16[16,16,1024]{2,1,0:T(8,128)(2,1)} %get-tuple-element.21, bf16[64,1024]{1,0:T(8,128)(2,1)S(1)} %copy-done.10, bf16[64,16]{0,1:T(8,128)(2,1)S(1)} %copy.42, f32[64,16]{0,1:T(8,128)S(1)} %convolution_select_fusion, f32[16]{0:T(128)S(1)} %iota_add_fusion), kind=kOutput, calls=%fused_computation.18 | convolution fusion | flops 33718272 | bytes 923712 | tf_op jit(solution)/shard_map/dot_general | solution.py:457
  105.3 1.1 copy.45
  106.3 3.7 %fusion.15 = bf16[64,1024]{1,0:T(8,128)(2,1)} fusion(f32[64,1024]{1,0:T(8,128)S(1)} %fusion.14, bf16[2048,1024]{1,0:T(8,128)(2,1)} %param.49, bf16[8,8,16,128]{3,2,1,0:T(8,128)(2,1)S(1)} %bitcast.91, f32[64]{0:T(128)S(1)} %slice_reduce_fusion), kind=kOutput, calls=%fused_computation.19 | convolution fusion | flops 268632064 | bytes 4849920 | tf_op jit(solution)/shard_map/dot_general | solution.py:461
  (17 shorter events, 0.0 us)
Async XLA Ops:
  0.6 74.8 %copy-start = (bf16[1,512,2048]{2,1,0:T(8,128)(2,1)S(1)}, bf16[1,512,2048]{2,1,0:T(8,128)(2,1)}, u32[]{:S(2)}) copy-start(bf16[1,512,2048]{2,1,0:T(8,128)(2,1)} %param.46) | copy-start | bytes 6291460
  20.9 3.5 %copy-start.2 = (bf16[1024,2048]{1,0:T(8,128)(2,1)S(1)}, bf16[1024,2048]{1,0:T(8,128)(2,1)}, u32[]{:S(2)}) copy-start(bf16[1024,2048]{1,0:T(8,128)(2,1)} %param.38) | copy-start | bytes 12582916
  20.9 3.5 %copy-start.7 = (bf16[64,1024]{1,0:T(8,128)(2,1)S(1)}, bf16[64,1024]{1,0:T(8,128)(2,1)}, u32[]{:S(2)}) copy-start(bf16[64,1024]{1,0:T(8,128)(2,1)} %get-tuple-element.14) | copy-start | bytes 393220
  24.4 36.7 %copy-start.8 = (bf16[1024,128]{1,0:T(8,128)(2,1)S(1)}, bf16[1024,128]{1,0:T(8,128)(2,1)}, u32[]{:S(2)}) copy-start(bf16[1024,128]{1,0:T(8,128)(2,1)} %param.48) | copy-start | bytes 786436
  25.3 38.3 %copy-start.9 = (bf16[1024,128]{1,0:T(8,128)(2,1)S(1)}, bf16[1024,128]{1,0:T(8,128)(2,1)}, u32[]{:S(2)}) copy-start(bf16[1024,128]{1,0:T(8,128)(2,1)} %param.47) | copy-start | bytes 786436
  61.1 2.5 %copy-start.1 = (bf16[4,2,2,64,1024]{4,3,2,1,0:T(8,128)(2,1)S(1)}, bf16[4,2,2,64,1024]{4,3,2,1,0:T(8,128)(2,1)}, u32[]{:S(2)}) copy-start(bf16[4,2,2,64,1024]{4,3,2,1,0:T(8,128)(2,1)} %get-tuple-element.18) | copy-start | bytes 6291460
  65.8 7.0 %copy-start.3 = (bf16[256,1024]{1,0:T(8,128)(2,1)S(1)}, bf16[256,1024]{1,0:T(8,128)(2,1)}, u32[]{:S(2)}) copy-start(bf16[256,1024]{1,0:T(8,128)(2,1)} %convolution_convert_fusion.3.refs_0_) | copy-start | bytes 1572868
  70.9 1.9 %copy-start.4 = (bf16[256,1024]{1,0:T(8,128)(2,1)S(1)}, bf16[256,1024]{1,0:T(8,128)(2,1)}, u32[]{:S(2)}) copy-start(bf16[256,1024]{1,0:T(8,128)(2,1)} %get-tuple-element.19) | copy-start | bytes 1572868
  70.9 3.0 %copy-start.11 = (bf16[1,2048,512]{2,1,0:T(8,128)(2,1)S(1)}, bf16[1,2048,512]{2,1,0:T(8,128)(2,1)}, u32[]{:S(2)}) copy-start(bf16[1,2048,512]{2,1,0:T(8,128)(2,1)} %param.44) | copy-start | bytes 6291460
  72.9 0.8 copy-start.5
  72.9 1.0 copy-start.6
  78.7 25.2 %copy-start.10 = (bf16[64,1024]{1,0:T(8,128)(2,1)S(1)}, bf16[64,1024]{1,0:T(8,128)(2,1)}, u32[]{:S(2)}) copy-start(bf16[64,1024]{1,0:T(8,128)(2,1)} %get-tuple-element.15) | copy-start | bytes 393220
